TPU v7x, 32 devices: a whole 2x2x4 slice. The times are simulated.
32 devices in a mesh: kv: 8 (over z, y), tp: 4 (over x, core).
Axes of the slice: x: 2, y: 2, z: 4, core: 2. Of those that a mesh axis runs over, the one named last changes fastest.
Arguments:
- queries: bfloat16 [2048, 3072], P('kv', 'tp'), may hold values from -6 to 6
- key_vectors: bfloat16 [2048, 512], P('kv', 'tp'), may hold values from -6 to 6
- value_vectors: bfloat16 [2048, 512], P('kv', 'tp'), may hold values from -6 to 6
- log_sums: float32 [2048, 48], P('kv', 'tp'), may hold values from 4.5 to 6.5
- out_grad: bfloat16 [2048, 3072], P('kv', 'tp'), may hold values from -48 to 48
- layer_input: bfloat16 [2048, 3072], P('kv', 'tp'), may hold values from -0.29882812 to 0.29882812
- chosen: int32 [32, 16], P('kv'), may hold values from -1 to 55, as said below
Outputs:
- query_grad: bfloat16 [2048, 3072], P('kv', 'tp')
- key_grad: bfloat16 [2048, 512], P('kv', 'tp')
- value_grad: bfloat16 [2048, 512], P('kv', 'tp')
- weight_grad: float32 [3072, 512], P('kv', 'tp')
Inputs may be any that keep to these rules, and one draw needn't show every extreme that they name: `chosen`: each entry is -1 or the number c of a block of 32 positions (c * 32 to c * 32 + 31) that lies wholly within an earlier index of kv than its query block. The numbers of one row differ, and all query blocks held by one index of kv together take at most one block from each other index.
All inputs are finite; a program needn't handle non-finite values.
Results may differ from a plain program's by a relative error of at most 0.0061.
Values may be sent and summed in bfloat16 or wider, within the bound.
A program may use at most 64 MiB of HBM per device.

v0:
```python
import functools

import jax
import jax.numpy as jnp
from jax import lax
from jax.experimental import pallas as pl
from jax.experimental.pallas import tpu as pltpu
from jax.sharding import PartitionSpec as P

HEAD = 64
KB = 32
QB = 64
NSEL = 16
MASKED = -1e30
SPREAD_AT = 7
MESH = pl.DeviceIdType.MESH


def dot_nt(a, b):
    return lax.dot_general(a, b, (((1,), (1,)), ((), ())), preferred_element_type=jnp.float32)


def dot_nn(a, b):
    return lax.dot_general(a, b, (((1,), (0,)), ((), ())), preferred_element_type=jnp.float32)


def dot_tn(a, b):
    return lax.dot_general(a, b, (((0,), (0,)), ((), ())), preferred_element_type=jnp.float32)


def padded_heads(pair, dst, scale):
    rows = pair.shape[0]
    wide = pair.astype(jnp.float32) * scale
    turned = pltpu.roll(wide, HEAD, 1)
    low = lax.broadcasted_iota(jnp.int32, wide.shape, 1) < HEAD
    zero = jnp.zeros_like(wide)
    dst[0, :rows] = jnp.where(low, wide, zero).astype(dst.dtype)
    dst[0, rows:] = jnp.where(low, zero, turned).astype(dst.dtype)
    dst[1, :rows] = jnp.where(low, turned, zero).astype(dst.dtype)
    dst[1, rows:] = jnp.where(low, zero, wide).astype(dst.dtype)


def folded_heads(totals, rows):
    low = lax.broadcasted_iota(jnp.int32, (rows, 2 * HEAD), 1) < HEAD
    first = totals[0, :rows] + pltpu.roll(totals[0, rows:], HEAD, 1)
    second = totals[1, rows:] + pltpu.roll(totals[1, :rows], HEAD, 1)
    return jnp.where(low, first, second)


def kernel(
    n_kv, n_tp,
    q_hbm, k_hbm, v_hbm, lse_hbm, do_hbm, x_ref, chosen_hbm,
    dq_ref, dk_ref, dv_ref, dw_ref,
    q_ref, do_ref, k_ref, v_ref, lse_ref, chosen_ref, lse_cols, asked, outgoing, fetched, ret_out, ret_in, x_mid, x_all, kg_all,
    k_own, v_own, k_sel, v_sel, bias_own, bias_sel, p_own, dp_own, o_own, delta, dq_part,
    dk_acc, dv_acc, dks_acc, dvs_acc, picks,
    ask_s, ask_r, blk_s, blk_r, ret_s, ret_r, x1_s, x1_r, x2_s, x2_r, x3_s, xt_s, xt_r, kg_s, kg_r, kgf_s, in_s,
):
    me = lax.axis_index("kv")
    col = lax.axis_index("tp")
    rows = q_ref.shape[0]
    width = k_ref.shape[1]
    pairs = q_ref.shape[1] // width
    per_head = pairs // 2
    here = rows // KB
    q_blocks = rows // QB
    sel_rows = n_kv * KB
    feats = dw_ref.shape[0]
    per_tp = x_ref.shape[1] // feats
    part = rows // n_tp
    devices = n_kv * n_tp
    mate = me + 1 - 2 * lax.rem(me, 2)
    twin = col + 1 - 2 * lax.rem(col, 2)
    score_scale = HEAD ** (-0.5)

    loads = [
        pltpu.make_async_copy(src, dst, in_s.at[n])
        for n, (src, dst) in enumerate(
            [
                (chosen_hbm, chosen_ref), (k_hbm, k_ref), (v_hbm, v_ref),
                (lse_hbm, lse_ref), (q_hbm, q_ref), (do_hbm, do_ref),
            ]
        )
    ]
    for load in loads:
        load.start()
    asked[...] = jnp.full(asked.shape, -1, jnp.int32)
    fetched[...] = jnp.zeros_like(fetched)
    ret_in[...] = jnp.zeros_like(ret_in)

    barrier = pltpu.get_barrier_semaphore()
    lin = me * n_tp + col

    def greet(d, carry):
        other = lax.rem(lin + d, devices)
        pl.semaphore_signal(
            barrier, inc=1, device_id={"kv": other // n_tp, "tp": lax.rem(other, n_tp)}, device_id_type=MESH
        )
        return carry

    lax.fori_loop(1, devices, greet, 0)

    def copy_to(src, dst, s_sem, r_sem, kv=None, tp=None):
        target = {"kv": me if kv is None else kv, "tp": col if tp is None else tp}
        return pltpu.make_async_remote_copy(
            src_ref=src, dst_ref=dst, send_sem=s_sem, recv_sem=r_sem,
            device_id=target, device_id_type=MESH,
        )

    def ask_copy(o):
        return copy_to(asked.at[me], asked.at[me], ask_s.at[o], ask_r.at[me], kv=o)

    def block_copy(p):
        return copy_to(outgoing.at[p], fetched.at[me], blk_s.at[p], blk_r.at[me], kv=p)

    def return_copy(o):
        return copy_to(ret_out.at[o], ret_in.at[me], ret_s.at[o], ret_r.at[me], kv=o)

    def grad_copy(p):
        return copy_to(kg_all.at[me], kg_all.at[me], kg_s.at[p], kg_r.at[me], kv=p)

    def forward_grad(p):
        return copy_to(kg_all.at[p], kg_all.at[p], kgf_s.at[p], kg_r.at[p], kv=mate)

    def quarter(c):
        return x_all.at[:, pl.ds(pl.multiple_of(c * part, part), part), :]

    def spread_copy(c):
        return copy_to(quarter(col), quarter(col), x2_s.at[c], x2_r.at[col], tp=c)

    def forward_copy(c):
        return copy_to(quarter(c), quarter(c), x3_s.at[c], x2_r.at[c], tp=twin)

    def sends_spread(c):
        return (c != col) & ((lax.rem(c, 2) == lax.rem(col, 2)) | (c == twin))

    def same_core(c):
        return (c != col) & (lax.rem(c, 2) == lax.rem(col, 2))

    def same_line(p):
        return (p != me) & (lax.rem(p, 2) == lax.rem(me, 2))

    def cross_copy(c):
        src = x_ref.at[pl.ds(c * part, part), :]
        return copy_to(src, x_mid.at[col], xt_s.at[c], xt_r.at[col], tp=c)

    def line_parts(i):
        src = x_mid.at[i // per_tp, :, pl.ds((i % per_tp) * feats, feats)]
        dst = x_all.at[me, pl.ds(pl.multiple_of(col * part, part), part), :]
        return src, dst

    def line_copy(i):
        src, dst = line_parts(i)
        return copy_to(src, dst, x1_s.at[i], x1_r.at[me], kv=i)

    def cross_own(c):
        return pltpu.make_async_copy(x_ref.at[pl.ds(c * part, part), :], x_mid.at[c], xt_r.at[c])

    def start_cross():
        for c in range(n_tp):
            @pl.when(c != col)
            def _(c=c):
                cross_copy(c).start()

            @pl.when(c == col)
            def _(c=c):
                cross_own(c).start()

    def start_line():
        for c in range(n_tp):
            @pl.when(c != col)
            def _(c=c):
                copy_to(x_mid.at[c], x_mid.at[c], xt_s.at[c], xt_r.at[c], tp=c).wait_recv()

            @pl.when(c == col)
            def _(c=c):
                cross_own(c).wait()
        for i in range(n_kv):
            src, dst = line_parts(i)

            @pl.when(i != me)
            def _(i=i):
                line_copy(i).start()

            @pl.when(i == me)
            def _(src=src, dst=dst, i=i):
                pltpu.make_async_copy(src, dst, x1_r.at[i]).start()

    def start_spread():
        for p in range(n_kv):
            piece = x_all.at[p, pl.ds(pl.multiple_of(col * part, part), part), :]
            pltpu.make_async_copy(piece, piece, x1_r.at[p]).wait()
        for c in range(n_tp):
            @pl.when(sends_spread(c))
            def _(c=c):
                spread_copy(c).start()

    for load in loads:
        load.wait()
    asked[me, :q_blocks, :NSEL] = chosen_ref[...]

    padded_heads(k_ref[...], k_own, score_scale)
    padded_heads(v_ref[...], v_own, 1.0)
    q_pos = lax.broadcasted_iota(jnp.int32, (rows, rows), 0)
    k_pos = lax.broadcasted_iota(jnp.int32, (rows, rows), 1)
    bias_own[...] = jnp.where(k_pos <= q_pos, 0.0, MASKED)
    sel_col = lax.broadcasted_iota(jnp.int32, (q_blocks, sel_rows), 1)
    first_of = (sel_col // KB) * here
    hit = jnp.zeros((q_blocks, sel_rows), jnp.int32)
    for j in range(NSEL):
        entry = chosen_ref[:, j : j + 1]
        hit = jnp.maximum(hit, jnp.where((entry >= first_of) & (entry < first_of + here), 1, 0))
    bias_rows = jnp.where(hit > 0, 0.0, MASKED)
    for b in range(q_blocks):
        bias_sel[b * QB : (b + 1) * QB, :] = jnp.broadcast_to(bias_rows[b : b + 1, :], (QB, sel_rows))

    def lanes(m):
        return slice(m * width, (m + 1) * width)

    def weights(scores, m, bias, keys):
        first = jnp.exp(scores[:, :keys] - lse_cols[:, 2 * m : 2 * m + 1] + bias)
        second = jnp.exp(scores[:, keys:] - lse_cols[:, 2 * m + 1 : 2 * m + 2] + bias)
        return first, second

    def own_pair(m):
        h = m // per_head
        do2 = do_ref[:, lanes(m)]
        first, second = weights(dot_nt(q_ref[:, lanes(m)], k_own[h]), m, bias_own[...], rows)
        p_own[m, :, :rows] = first
        p_own[m, :, rows:] = second
        p16 = jnp.concatenate([first.astype(jnp.bfloat16), second.astype(jnp.bfloat16)], axis=1)
        dp_own[m] = dot_nt(do2, v_own[h])
        o_own[m] = dot_nn(p16, v_own[h])
        term = dot_tn(p16, do2)
        if m % per_head == 0:
            dv_acc[h] = term
        else:
            dv_acc[h] += term

    def sel_pair(m):
        h = m // per_head
        do2 = do_ref[:, lanes(m)]
        q2 = q_ref[:, lanes(m)]
        first, second = weights(dot_nt(q2, k_sel[h]), m, bias_sel[...], sel_rows)
        p16 = jnp.concatenate([first.astype(jnp.bfloat16), second.astype(jnp.bfloat16)], axis=1)
        dp = dot_nt(do2, v_sel[h])
        prod = do2.astype(jnp.float32) * (o_own[m] + dot_nn(p16, v_sel[h]))
        low = lax.broadcasted_iota(jnp.int32, prod.shape, 1) < HEAD
        d_first = jnp.sum(jnp.where(low, prod, 0.0), axis=1, keepdims=True)
        d_second = jnp.sum(jnp.where(low, 0.0, prod), axis=1, keepdims=True)
        delta[m] = jnp.where(low, d_first, d_second)
        ds = jnp.concatenate(
            [
                (first * (dp[:, :sel_rows] - d_first)).astype(jnp.bfloat16),
                (second * (dp[:, sel_rows:] - d_second)).astype(jnp.bfloat16),
            ],
            axis=1,
        )
        dq_part[m] = dot_nn(ds, k_sel[h])
        k_term = dot_tn(ds, q2)
        v_term = dot_tn(p16, do2)
        if m % per_head == 0:
            dks_acc[h] = k_term
            dvs_acc[h] = v_term
        else:
            dks_acc[h] += k_term
            dvs_acc[h] += v_term

    def own_pair_back(m):
        h = m // per_head
        d_first = delta[m, :, 0:1]
        d_second = delta[m, :, HEAD : HEAD + 1]
        ds = jnp.concatenate(
            [
                (p_own[m, :, :rows] * (dp_own[m, :, :rows] - d_first)).astype(jnp.bfloat16),
                (p_own[m, :, rows:] * (dp_own[m, :, rows:] - d_second)).astype(jnp.bfloat16),
            ],
            axis=1,
        )
        dq_ref[:, lanes(m)] = (dq_part[m] + dot_nn(ds, k_own[h])).astype(dq_ref.dtype)
        term = dot_tn(ds, q_ref[:, lanes(m)])
        if m % per_head == 0:
            dk_acc[h] = term
        else:
            dk_acc[h] += term

    lse_cols[...] = jnp.transpose(lse_ref[...])
    cuts = (pairs // 3, 2 * pairs // 3)
    for m in range(cuts[0]):
        own_pair(m)

    pl.semaphore_wait(barrier, devices - 1)
    for o in range(n_kv):
        @pl.when(o < me)
        def _(o=o):
            ask_copy(o).start()
    start_cross()

    for m in range(cuts[0], cuts[1]):
        own_pair(m)

    for p in range(n_kv):
        @pl.when(p > me)
        def _(p=p):
            copy_to(asked.at[p], asked.at[p], ask_s.at[p], ask_r.at[p], kv=p).wait_recv()

    wants = asked[...]
    mine = (wants >= me * here) & (wants < me * here + here)
    local = jnp.where(mine, wants - me * here, -1)
    local = jnp.max(jnp.max(local, axis=2, keepdims=True), axis=1, keepdims=True)
    shape = (n_kv, KB, rows)
    at = lax.broadcasted_iota(jnp.int32, shape, 2)
    offset = lax.broadcasted_iota(jnp.int32, shape, 1)
    sender = lax.broadcasted_iota(jnp.int32, shape, 0)
    chosen_here = (local >= 0) & (sender > me) & (at == local * KB + offset)
    picks[...] = jnp.where(chosen_here, 1.0, 0.0).astype(jnp.bfloat16).reshape(sel_rows, rows)
    outgoing[:, :, :width] = dot_nn(picks[...], k_ref[...]).astype(jnp.bfloat16).reshape(n_kv, KB, width)
    outgoing[:, :, width:] = dot_nn(picks[...], v_ref[...]).astype(jnp.bfloat16).reshape(n_kv, KB, width)
    for p in range(n_kv):
        @pl.when(p > me)
        def _(p=p):
            block_copy(p).start()

    for m in range(cuts[1], pairs):
        own_pair(m)

    start_line()
    for o in range(n_kv):
        @pl.when(o < me)
        def _(o=o):
            copy_to(fetched.at[o], fetched.at[o], blk_s.at[o], blk_r.at[o], kv=o).wait_recv()

    got = fetched[...].reshape(sel_rows, 2 * width)
    padded_heads(got[:, :width], k_sel, score_scale)
    padded_heads(got[:, width:], v_sel, 1.0)
    for m in range(pairs):
        if m == SPREAD_AT:
            start_spread()
        sel_pair(m)

    ret_out[:, :, :width] = (
        (folded_heads(dks_acc, sel_rows) * score_scale).astype(ret_out.dtype).reshape(n_kv, KB, width)
    )
    ret_out[:, :, width:] = folded_heads(dvs_acc, sel_rows).astype(ret_out.dtype).reshape(n_kv, KB, width)
    for o in range(n_kv):
        @pl.when(o < me)
        def _(o=o):
            return_copy(o).start()
    if SPREAD_AT == pairs:
        start_spread()
    for m in range(pairs):
        own_pair_back(m)
    if SPREAD_AT == pairs + 1:
        start_spread()

    for p in range(n_kv):
        @pl.when(p > me)
        def _(p=p):
            copy_to(ret_in.at[p], ret_in.at[p], ret_s.at[p], ret_r.at[p], kv=p).wait_recv()

    landed = dot_tn(picks[...], ret_in[...].reshape(sel_rows, 2 * width))
    key_grad = (folded_heads(dk_acc, rows) * score_scale + landed[:, :width]).astype(jnp.bfloat16)
    kg_all[me] = key_grad
    for p in range(n_kv):
        @pl.when(same_line(p) | (p == mate))
        def _(p=p):
            grad_copy(p).start()
    dk_ref[...] = key_grad
    dv_ref[...] = (folded_heads(dv_acc, rows) + landed[:, width:]).astype(jnp.bfloat16)

    for c in range(n_tp):
        @pl.when(same_core(c))
        def _(c=c):
            copy_to(quarter(c), quarter(c), x2_s.at[c], x2_r.at[c], tp=c).wait_recv()
            forward_copy(c).start()

    for p in range(n_kv):
        @pl.when(same_line(p))
        def _(p=p):
            copy_to(kg_all.at[p], kg_all.at[p], kg_s.at[p], kg_r.at[p], kv=p).wait_recv()
            forward_grad(p).start()

    for c in range(n_tp):
        @pl.when((c != col) & jnp.logical_not(same_core(c)))
        def _(c=c):
            copy_to(quarter(c), quarter(c), x2_s.at[c], x2_r.at[c], tp=c).wait_recv()

    total = None
    for step in range(n_kv // 2):
        p = lax.rem(me + 2 * step, n_kv)
        term = dot_tn(x_all[p], kg_all[p])
        total = term if total is None else total + term
    dw_ref[...] = total
    for p in range(n_kv):
        @pl.when((p != me) & jnp.logical_not(same_line(p)))
        def _(p=p):
            copy_to(kg_all.at[p], kg_all.at[p], kg_s.at[p], kg_r.at[p], kv=p).wait_recv()
    total = dw_ref[...]
    for step in range(n_kv // 2):
        p = lax.rem(mate + 2 * step, n_kv)
        total = total + dot_tn(x_all[p], kg_all[p])
    dw_ref[...] = total

    for o in range(n_kv):
        @pl.when(o < me)
        def _(o=o):
            ask_copy(o).wait_send()
            return_copy(o).wait_send()

        @pl.when(o > me)
        def _(o=o):
            block_copy(o).wait_send()

        @pl.when(same_line(o) | (o == mate))
        def _(o=o):
            grad_copy(o).wait_send()

        @pl.when(same_line(o))
        def _(o=o):
            forward_grad(o).wait_send()

    for i in range(n_kv):
        @pl.when(i != me)
        def _(i=i):
            line_copy(i).wait_send()

    for c in range(n_tp):
        @pl.when(c != col)
        def _(c=c):
            cross_copy(c).wait_send()

    for c in range(n_tp):
        @pl.when(sends_spread(c))
        def _(c=c):
            spread_copy(c).wait_send()

        @pl.when(same_core(c))
        def _(c=c):
            forward_copy(c).wait_send()


def per_device_fused(queries, key_vectors, value_vectors, log_sums, out_grad, layer_input, chosen):
    n_kv = lax.axis_size("kv")
    n_tp = lax.axis_size("tp")
    rows, features = queries.shape
    width = key_vectors.shape[1]
    pairs = features // width
    sel_rows = n_kv * KB
    feats = layer_input.shape[1] * n_tp // n_kv
    per_tp = layer_input.shape[1] // feats
    f32, bf16 = jnp.float32, jnp.bfloat16
    dma = pltpu.SemaphoreType.DMA
    vmem = pl.BlockSpec(memory_space=pltpu.VMEM)
    hbm = pl.BlockSpec(memory_space=pl.ANY)
    scratch = [
        pltpu.VMEM((rows, features), bf16),
        pltpu.VMEM((rows, features), bf16),
        pltpu.VMEM((rows, width), bf16),
        pltpu.VMEM((rows, width), bf16),
        pltpu.VMEM((log_sums.shape[1], rows), f32),
        pltpu.VMEM(chosen.shape, jnp.int32),
        pltpu.VMEM((rows, log_sums.shape[1]), f32),
        pltpu.VMEM((n_kv, 8, 128), jnp.int32),
        pltpu.VMEM((n_kv, KB, 2 * width), bf16),
        pltpu.VMEM((n_kv, KB, 2 * width), bf16),
        pltpu.VMEM((n_kv, KB, 2 * width), bf16),
        pltpu.VMEM((n_kv, KB, 2 * width), bf16),
        pltpu.VMEM((n_tp, rows // n_tp, layer_input.shape[1]), bf16),
        pltpu.VMEM((n_kv, rows, feats), bf16),
        pltpu.VMEM((n_kv, rows, width), bf16),
        pltpu.VMEM((2, 2 * rows, width), bf16),
        pltpu.VMEM((2, 2 * rows, width), bf16),
        pltpu.VMEM((2, 2 * sel_rows, width), bf16),
        pltpu.VMEM((2, 2 * sel_rows, width), bf16),
        pltpu.VMEM((rows, rows), f32),
        pltpu.VMEM((rows, sel_rows), f32),
        pltpu.VMEM((pairs, rows, 2 * rows), f32),
        pltpu.VMEM((pairs, rows, 2 * rows), f32),
        pltpu.VMEM((pairs, rows, width), f32),
        pltpu.VMEM((pairs, rows, width), f32),
        pltpu.VMEM((pairs, rows, width), f32),
        pltpu.VMEM((2, 2 * rows, width), f32),
        pltpu.VMEM((2, 2 * rows, width), f32),
        pltpu.VMEM((2, 2 * sel_rows, width), f32),
        pltpu.VMEM((2, 2 * sel_rows, width), f32),
        pltpu.VMEM((sel_rows, rows), bf16),
    ] + [dma((n_kv,))] * 6 + [dma((n_kv,))] * 2 + [dma((n_tp,))] * 5 + [dma((n_kv,))] * 3 + [dma((6,))]
    return pl.pallas_call(
        functools.partial(kernel, n_kv, n_tp),
        out_shape=(
            jax.ShapeDtypeStruct((rows, features), bf16),
            jax.ShapeDtypeStruct((rows, width), bf16),
            jax.ShapeDtypeStruct((rows, width), bf16),
            jax.ShapeDtypeStruct((feats, width), f32),
        ),
        in_specs=[hbm] * 7,
        out_specs=(vmem,) * 4,
        scratch_shapes=scratch,
        compiler_params=pltpu.CompilerParams(
            collective_id=0, has_side_effects=True
        ),
    )(queries, key_vectors, value_vectors, log_sums.T, out_grad, layer_input, chosen)


def fits_fused(n_kv, n_tp, rows, features, width, x_features):
    if (x_features * n_tp) % n_kv or width != 2 * HEAD or features % (6 * width):
        return False
    feats = x_features * n_tp // n_kv
    whole_tiles = feats % 128 == 0 and x_features % feats == 0 and rows % (16 * n_tp) == 0
    return whole_tiles and rows // QB <= 8 and n_kv * KB <= 512 and n_kv % 2 == 0 and n_tp % 2 == 0


def per_device(queries, key_vectors, value_vectors, log_sums, out_grad, layer_input, chosen):
    fused = fits_fused(
        lax.axis_size("kv"), lax.axis_size("tp"), queries.shape[0], queries.shape[1],
        key_vectors.shape[1], layer_input.shape[1],
    )
    run = per_device_fused if fused else per_device_general
    return run(queries, key_vectors, value_vectors, log_sums, out_grad, layer_input, chosen)


def per_device_general(queries, key_vectors, value_vectors, log_sums, out_grad, layer_input, chosen):
    axis_count = lax.axis_size("kv")
    own_index = lax.axis_index("kv")
    span_rows = queries.shape[0]
    kv_local = key_vectors.shape[1] // HEAD
    group_size = queries.shape[1] // key_vectors.shape[1]
    blocks_here = span_rows // KB
    query_blocks = span_rows // QB
    score_scale = HEAD ** (-0.5)
    half_width = kv_local * HEAD
    pair_width = 2 * half_width
    paired = jnp.concatenate([key_vectors, value_vectors], axis=1)
    owners = jnp.arange(axis_count, dtype=jnp.int32)
    usable = chosen >= 0
    owner_of = jnp.where(usable, chosen // blocks_here, -1)
    within = chosen - chosen // blocks_here * blocks_here
    matched = owner_of[:, :, None] == owners[None, None, :]
    wanted = jnp.max(jnp.where(matched, within[:, :, None], -1), axis=(0, 1))
    incoming = lax.all_to_all(wanted[:, None], "kv", split_axis=0, concat_axis=0, tiled=True)[:, 0]
    blocks = paired.reshape(blocks_here, KB, pair_width)
    outgoing = jnp.where(
        (incoming >= 0)[:, None, None],
        blocks[jnp.maximum(incoming, 0)],
        jnp.zeros((), paired.dtype),
    )
    fetched = lax.all_to_all(outgoing, "kv", split_axis=0, concat_axis=0, tiled=True)
    query_parts = queries.reshape(query_blocks, QB, kv_local, group_size, HEAD)
    grad_parts = out_grad.reshape(query_blocks, QB, kv_local, group_size, HEAD)
    sum_parts = log_sums.reshape(query_blocks, QB, kv_local, group_size)
    slot_owner = jnp.clip(owner_of, 0, axis_count - 1)
    key_own = key_vectors.reshape(span_rows, kv_local, HEAD)
    value_own = value_vectors.reshape(span_rows, kv_local, HEAD)
    key_pos = own_index * span_rows + jnp.arange(span_rows, dtype=jnp.int32)

    def one_block(packed):
        query_part, grad_part, sum_part, slot_part, usable_part, block_index = packed
        selected = fetched[slot_part].reshape(NSEL * KB, 2, kv_local, HEAD)
        key_sel = selected[:, 0]
        value_sel = selected[:, 1]
        keep_key = jnp.repeat(usable_part, KB)
        query_pos = own_index * span_rows + block_index * QB + jnp.arange(QB, dtype=jnp.int32)
        causal = key_pos[None, :] <= query_pos[:, None]
        score_sel = (
            jnp.einsum("qhgd,khd->qhgk", query_part, key_sel, preferred_element_type=jnp.float32)
            * score_scale
        )
        score_own = (
            jnp.einsum("qhgd,khd->qhgk", query_part, key_own, preferred_element_type=jnp.float32)
            * score_scale
        )
        weight_sel = jnp.where(
            keep_key[None, None, None, :], jnp.exp(score_sel - sum_part[..., None]), 0.0
        )
        weight_own = jnp.where(
            causal[:, None, None, :], jnp.exp(score_own - sum_part[..., None]), 0.0
        )
        round_sel = weight_sel.astype(jnp.bfloat16)
        round_own = weight_own.astype(jnp.bfloat16)
        output = jnp.einsum(
            "qhgk,khd->qhgd", round_sel, value_sel, preferred_element_type=jnp.float32
        )
        output = output + jnp.einsum(
            "qhgk,khd->qhgd", round_own, value_own, preferred_element_type=jnp.float32
        )
        row_delta = jnp.sum(grad_part.astype(jnp.float32) * output, axis=-1)
        prod_sel = jnp.einsum(
            "qhgd,khd->qhgk", grad_part, value_sel, preferred_element_type=jnp.float32
        )
        prod_own = jnp.einsum(
            "qhgd,khd->qhgk", grad_part, value_own, preferred_element_type=jnp.float32
        )
        slope_sel = (weight_sel * (prod_sel - row_delta[..., None])).astype(jnp.bfloat16)
        slope_own = (weight_own * (prod_own - row_delta[..., None])).astype(jnp.bfloat16)
        query_total = jnp.einsum(
            "qhgk,khd->qhgd", slope_sel, key_sel, preferred_element_type=jnp.float32
        )
        query_total = query_total + jnp.einsum(
            "qhgk,khd->qhgd", slope_own, key_own, preferred_element_type=jnp.float32
        )
        query_out = (query_total * score_scale).astype(jnp.bfloat16)
        key_sel_grad = (
            jnp.einsum("qhgk,qhgd->khd", slope_sel, query_part, preferred_element_type=jnp.float32)
            * score_scale
        )
        value_sel_grad = jnp.einsum(
            "qhgk,qhgd->khd", round_sel, grad_part, preferred_element_type=jnp.float32
        )
        key_own_grad = (
            jnp.einsum("qhgk,qhgd->khd", slope_own, query_part, preferred_element_type=jnp.float32)
            * score_scale
        )
        value_own_grad = jnp.einsum(
            "qhgk,qhgd->khd", round_own, grad_part, preferred_element_type=jnp.float32
        )
        sel_pair = jnp.concatenate(
            [
                key_sel_grad.reshape(NSEL, KB, half_width),
                value_sel_grad.reshape(NSEL, KB, half_width),
            ],
            axis=2,
        )
        own_pair = jnp.concatenate(
            [
                key_own_grad.reshape(span_rows, half_width),
                value_own_grad.reshape(span_rows, half_width),
            ],
            axis=1,
        )
        return (query_out, sel_pair, own_pair)

    block_ids = jnp.arange(query_blocks, dtype=jnp.int32)
    query_outs, sel_pairs, own_pairs = lax.map(
        one_block, (query_parts, grad_parts, sum_parts, slot_owner, usable, block_ids)
    )
    onehot = ((slot_owner[:, :, None] == owners[None, None, :]) & usable[:, :, None]).astype(
        jnp.float32
    )
    onehot = onehot.reshape(query_blocks * NSEL, axis_count)
    per_owner = jnp.einsum(
        "so,sr->or",
        onehot,
        sel_pairs.reshape(query_blocks * NSEL, KB * pair_width),
        precision=lax.Precision.HIGHEST,
    )
    returned = lax.all_to_all(
        per_owner.reshape(axis_count, KB, pair_width), "kv", split_axis=0, concat_axis=0, tiled=True
    )
    placing = (incoming[None, :] == jnp.arange(blocks_here, dtype=jnp.int32)[:, None]).astype(
        jnp.float32
    )
    landed = jnp.einsum(
        "bs,sr->br",
        placing,
        returned.reshape(axis_count, KB * pair_width),
        precision=lax.Precision.HIGHEST,
    )
    totals = jnp.sum(own_pairs, axis=0) + landed.reshape(span_rows, pair_width)
    key_grad = totals[:, :half_width].astype(jnp.bfloat16)
    value_grad = totals[:, half_width:].astype(jnp.bfloat16)
    full_input = lax.all_gather(layer_input, "tp", axis=1, tiled=True)
    weight_grad = lax.psum_scatter(
        lax.dot_general(
            full_input, key_grad, (((0,), (0,)), ((), ())), preferred_element_type=jnp.float32
        ),
        "kv",
        scatter_dimension=0,
        tiled=True,
    )
    return (query_outs.reshape(span_rows, queries.shape[1]), key_grad, value_grad, weight_grad)


def solution(mesh):
    placed = (
        P("kv", "tp"),
        P("kv", "tp"),
        P("kv", "tp"),
        P("kv", "tp"),
        P("kv", "tp"),
        P("kv", "tp"),
        P("kv", None),
    )
    return jax.shard_map(
        per_device,
        mesh=mesh,
        in_specs=placed,
        out_specs=(P("kv", "tp"), P("kv", "tp"), P("kv", "tp"), P("kv", "tp")),
        check_vma=False,
    )
```

profile of v0, /device:TPU:8, one launch (start us, length us, event | category | flops | bytes accessed | tf_op | source)
XLA Modules:
  0.0 45.0 jit_solution(16480472940062399841)
XLA Ops:
  0.6 40.6 %shard_map.102 = (bf16[256,768]{1,0:T(8,128)(2,1)}, bf16[256,128]{1,0:T(8,128)(2,1)}, bf16[256,128]{1,0:T(8,128)(2,1)}, f32[384,128]{1,0:T(8,128)}) custom-call(bf16[256,768]{1,0:T(8,128)(2,1)} %q_hbm.1, bf16[256,128]{1,0:T(8,128)(2,1)} %k_hbm.1, bf16[256,128]{1,0:T(8,128)(2,1)} %v_hbm.1, f32[12,256]{1,0:T(8,128)} %bitcast.1, bf16[256,768]{1,0:T(8,128)(2,1)} %do_hbm.1, ...), custom_call_target="tpu_custom_call" | custom-call | tf_op jit(solution)/shard_map/pallas_call | solution.py:488
  41.2 0.0 copy-start.2
  41.3 0.0 copy-start.1
  41.3 1.8 %copy.15 = bf16[256,768]{1,0:T(8,128)(2,1)} copy(bf16[256,768]{1,0:T(8,128)(2,1)} %get-tuple-element.8) | data formatting | bytes 786432
  43.1 0.0 copy-done.2
  43.1 0.0 copy-start
  43.1 0.6 %copy.16 = bf16[256,128]{1,0:T(8,128)(2,1)} copy(bf16[256,128]{1,0:T(8,128)(2,1)S(1)} %copy-done.2) | data formatting | bytes 131072
  43.7 0.0 copy-done.1
  43.7 0.6 %copy.17 = bf16[256,128]{1,0:T(8,128)(2,1)} copy(bf16[256,128]{1,0:T(8,128)(2,1)S(1)} %copy-done.1) | data formatting | bytes 131072
  44.3 0.0 copy-done
  44.3 0.7 %copy.18 = f32[384,128]{1,0:T(8,128)} copy(f32[384,128]{1,0:T(8,128)S(1)} %copy-done) | data formatting | bytes 393216
Async XLA Ops:
  41.2 1.8 %copy-start.2 = (bf16[256,128]{1,0:T(8,128)(2,1)S(1)}, bf16[256,128]{1,0:T(8,128)(2,1)}, u32[]{:S(2)}) copy-start(bf16[256,128]{1,0:T(8,128)(2,1)} %get-tuple-element.9) | copy-start | bytes 196612
  41.3 2.4 %copy-start.1 = (bf16[256,128]{1,0:T(8,128)(2,1)S(1)}, bf16[256,128]{1,0:T(8,128)(2,1)}, u32[]{:S(2)}) copy-start(bf16[256,128]{1,0:T(8,128)(2,1)} %get-tuple-element.10) | copy-start | bytes 196612
  43.1 1.3 %copy-start = (f32[384,128]{1,0:T(8,128)S(1)}, f32[384,128]{1,0:T(8,128)}, u32[]{:S(2)}) copy-start(f32[384,128]{1,0:T(8,128)} %get-tuple-element.11) | copy-start | bytes 589828
where the time goes:
time: 45.2 us; the launch traced here: 45 us
  Pallas kernels  40.6 us (90%)
  local copies, waits for them, and re-layouts  3.75 us (8%)
  between operations  0.66 us (1%)
    pallas_call x1, Pallas kernels, per_device_fused(): pl.pallas_call(functools.partial(kernel, n_kv, n_tp), out_shape=(jax.Shap...  40.6 us
    unnamed x10, local copies, waits for them, and re-layouts  3.75 us

commit v1 on v0

--- a/solution.py
+++ b/solution.py
@@ -40,6 +40,10 @@
     dst[1, rows:] = jnp.where(low, zero, wide).astype(dst.dtype)
 
 
+def turned_keys(pair):
+    return jnp.transpose(pair.astype(jnp.float32) * HEAD ** (-0.5)).astype(jnp.bfloat16)
+
+
 def folded_heads(totals, rows):
     low = lax.broadcasted_iota(jnp.int32, (rows, 2 * HEAD), 1) < HEAD
     first = totals[0, :rows] + pltpu.roll(totals[0, rows:], HEAD, 1)
@@ -51,8 +55,8 @@
     n_kv, n_tp,
     q_hbm, k_hbm, v_hbm, lse_hbm, do_hbm, x_ref, chosen_hbm,
     dq_ref, dk_ref, dv_ref, dw_ref,
-    q_ref, do_ref, k_ref, v_ref, lse_ref, chosen_ref, lse_cols, asked, outgoing, fetched, ret_out, ret_in, x_mid, x_all, kg_all,
-    k_own, v_own, k_sel, v_sel, bias_own, bias_sel, p_own, dp_own, o_own, delta, dq_part,
+    q_ref, do_ref, k_ref, v_ref, lse_ref, chosen_ref, asked, outgoing, fetched, ret_out, ret_in, x_mid, x_all, kg_all,
+    k_own, v_own, k_sel, v_sel, kt_own, kt_sel, bias_own, bias_sel, p_own, dp_own, delta, ds_sel,
     dk_acc, dv_acc, dks_acc, dvs_acc, picks,
     ask_s, ask_r, blk_s, blk_r, ret_s, ret_r, x1_s, x1_r, x2_s, x2_r, x3_s, xt_s, xt_r, kg_s, kg_r, kgf_s, in_s,
 ):
@@ -201,8 +205,9 @@
 
     padded_heads(k_ref[...], k_own, score_scale)
     padded_heads(v_ref[...], v_own, 1.0)
-    q_pos = lax.broadcasted_iota(jnp.int32, (rows, rows), 0)
-    k_pos = lax.broadcasted_iota(jnp.int32, (rows, rows), 1)
+    kt_own[...] = turned_keys(k_ref[...])
+    k_pos = lax.broadcasted_iota(jnp.int32, (rows, rows), 0)
+    q_pos = lax.broadcasted_iota(jnp.int32, (rows, rows), 1)
     bias_own[...] = jnp.where(k_pos <= q_pos, 0.0, MASKED)
     sel_col = lax.broadcasted_iota(jnp.int32, (q_blocks, sel_rows), 1)
     first_of = (sel_col // KB) * here
@@ -211,27 +216,33 @@
         entry = chosen_ref[:, j : j + 1]
         hit = jnp.maximum(hit, jnp.where((entry >= first_of) & (entry < first_of + here), 1, 0))
     bias_rows = jnp.where(hit > 0, 0.0, MASKED)
-    for b in range(q_blocks):
-        bias_sel[b * QB : (b + 1) * QB, :] = jnp.broadcast_to(bias_rows[b : b + 1, :], (QB, sel_rows))
+    in_block = lax.broadcasted_iota(jnp.int32, (q_blocks, rows), 1) // QB
+    spots = jnp.where(in_block == lax.broadcasted_iota(jnp.int32, (q_blocks, rows), 0), 1.0, 0.0)
+    bias_sel[...] = dot_tn(bias_rows, spots)
 
     def lanes(m):
         return slice(m * width, (m + 1) * width)
 
     def weights(scores, m, bias, keys):
-        first = jnp.exp(scores[:, :keys] - lse_cols[:, 2 * m : 2 * m + 1] + bias)
-        second = jnp.exp(scores[:, keys:] - lse_cols[:, 2 * m + 1 : 2 * m + 2] + bias)
+        first = jnp.exp(scores[:keys] - lse_ref[2 * m : 2 * m + 1, :] + bias)
+        second = jnp.exp(scores[keys:] - lse_ref[2 * m + 1 : 2 * m + 2, :] + bias)
         return first, second
+
+    def row_terms(p16, dp):
+        return jnp.sum(p16.astype(jnp.float32) * dp, axis=0, keepdims=True)
 
     def own_pair(m):
         h = m // per_head
         do2 = do_ref[:, lanes(m)]
-        first, second = weights(dot_nt(q_ref[:, lanes(m)], k_own[h]), m, bias_own[...], rows)
-        p_own[m, :, :rows] = first
-        p_own[m, :, rows:] = second
-        p16 = jnp.concatenate([first.astype(jnp.bfloat16), second.astype(jnp.bfloat16)], axis=1)
-        dp_own[m] = dot_nt(do2, v_own[h])
-        o_own[m] = dot_nn(p16, v_own[h])
-        term = dot_tn(p16, do2)
+        first, second = weights(dot_nt(k_own[h], q_ref[:, lanes(m)]), m, bias_own[...], rows)
+        p_own[m, :rows] = first
+        p_own[m, rows:] = second
+        dp = dot_nt(v_own[h], do2)
+        dp_own[m] = dp
+        first16, second16 = first.astype(jnp.bfloat16), second.astype(jnp.bfloat16)
+        delta[2 * m : 2 * m + 1, :] = row_terms(first16, dp[:rows])
+        delta[2 * m + 1 : 2 * m + 2, :] = row_terms(second16, dp[rows:])
+        term = dot_nn(jnp.concatenate([first16, second16], axis=0), do2)
         if m % per_head == 0:
             dv_acc[h] = term
         else:
@@ -241,24 +252,23 @@
         h = m // per_head
         do2 = do_ref[:, lanes(m)]
         q2 = q_ref[:, lanes(m)]
-        first, second = weights(dot_nt(q2, k_sel[h]), m, bias_sel[...], sel_rows)
-        p16 = jnp.concatenate([first.astype(jnp.bfloat16), second.astype(jnp.bfloat16)], axis=1)
-        dp = dot_nt(do2, v_sel[h])
-        prod = do2.astype(jnp.float32) * (o_own[m] + dot_nn(p16, v_sel[h]))
-        low = lax.broadcasted_iota(jnp.int32, prod.shape, 1) < HEAD
-        d_first = jnp.sum(jnp.where(low, prod, 0.0), axis=1, keepdims=True)
-        d_second = jnp.sum(jnp.where(low, 0.0, prod), axis=1, keepdims=True)
-        delta[m] = jnp.where(low, d_first, d_second)
+        first, second = weights(dot_nt(k_sel[h], q2), m, bias_sel[...], sel_rows)
+        dp = dot_nt(v_sel[h], do2)
+        first16, second16 = first.astype(jnp.bfloat16), second.astype(jnp.bfloat16)
+        d_first = delta[2 * m : 2 * m + 1, :] + row_terms(first16, dp[:sel_rows])
+        d_second = delta[2 * m + 1 : 2 * m + 2, :] + row_terms(second16, dp[sel_rows:])
+        delta[2 * m : 2 * m + 1, :] = d_first
+        delta[2 * m + 1 : 2 * m + 2, :] = d_second
         ds = jnp.concatenate(
             [
-                (first * (dp[:, :sel_rows] - d_first)).astype(jnp.bfloat16),
-                (second * (dp[:, sel_rows:] - d_second)).astype(jnp.bfloat16),
+                (first * (dp[:sel_rows] - d_first)).astype(jnp.bfloat16),
+                (second * (dp[sel_rows:] - d_second)).astype(jnp.bfloat16),
             ],
-            axis=1,
-        )
-        dq_part[m] = dot_nn(ds, k_sel[h])
-        k_term = dot_tn(ds, q2)
-        v_term = dot_tn(p16, do2)
+            axis=0,
+        )
+        ds_sel[m] = ds
+        k_term = dot_nn(ds, q2)
+        v_term = dot_nn(jnp.concatenate([first16, second16], axis=0), do2)
         if m % per_head == 0:
             dks_acc[h] = k_term
             dvs_acc[h] = v_term
@@ -268,23 +278,24 @@
 
     def own_pair_back(m):
         h = m // per_head
-        d_first = delta[m, :, 0:1]
-        d_second = delta[m, :, HEAD : HEAD + 1]
-        ds = jnp.concatenate(
-            [
-                (p_own[m, :, :rows] * (dp_own[m, :, :rows] - d_first)).astype(jnp.bfloat16),
-                (p_own[m, :, rows:] * (dp_own[m, :, rows:] - d_second)).astype(jnp.bfloat16),
-            ],
-            axis=1,
-        )
-        dq_ref[:, lanes(m)] = (dq_part[m] + dot_nn(ds, k_own[h])).astype(dq_ref.dtype)
-        term = dot_tn(ds, q_ref[:, lanes(m)])
+        head = slice(h * HEAD, (h + 1) * HEAD)
+        ds = []
+        dq = []
+        for j in range(2):
+            part_rows = slice(j * rows, (j + 1) * rows)
+            one = (p_own[m, part_rows] * (dp_own[m, part_rows] - delta[2 * m + j : 2 * m + j + 1, :])).astype(jnp.bfloat16)
+            ds.append(one)
+            dq.append(
+                dot_nn(kt_own[head, :], one)
+                + dot_nn(kt_sel[head, :], ds_sel[m, j * sel_rows : (j + 1) * sel_rows, :])
+            )
+        dq_ref[:, lanes(m)] = jnp.transpose(jnp.concatenate(dq, axis=0)).astype(dq_ref.dtype)
+        term = dot_nn(jnp.concatenate(ds, axis=0), q_ref[:, lanes(m)])
         if m % per_head == 0:
             dk_acc[h] = term
         else:
             dk_acc[h] += term
 
-    lse_cols[...] = jnp.transpose(lse_ref[...])
     cuts = (pairs // 3, 2 * pairs // 3)
     for m in range(cuts[0]):
         own_pair(m)
@@ -333,6 +344,7 @@
     got = fetched[...].reshape(sel_rows, 2 * width)
     padded_heads(got[:, :width], k_sel, score_scale)
     padded_heads(got[:, width:], v_sel, 1.0)
+    kt_sel[...] = turned_keys(got[:, :width])
     for m in range(pairs):
         if m == SPREAD_AT:
             start_spread()
@@ -459,7 +471,6 @@
         pltpu.VMEM((rows, width), bf16),
         pltpu.VMEM((log_sums.shape[1], rows), f32),
         pltpu.VMEM(chosen.shape, jnp.int32),
-        pltpu.VMEM((rows, log_sums.shape[1]), f32),
         pltpu.VMEM((n_kv, 8, 128), jnp.int32),
         pltpu.VMEM((n_kv, KB, 2 * width), bf16),
         pltpu.VMEM((n_kv, KB, 2 * width), bf16),
@@ -472,13 +483,14 @@
         pltpu.VMEM((2, 2 * rows, width), bf16),
         pltpu.VMEM((2, 2 * sel_rows, width), bf16),
         pltpu.VMEM((2, 2 * sel_rows, width), bf16),
+        pltpu.VMEM((width, rows), bf16),
+        pltpu.VMEM((width, sel_rows), bf16),
         pltpu.VMEM((rows, rows), f32),
-        pltpu.VMEM((rows, sel_rows), f32),
-        pltpu.VMEM((pairs, rows, 2 * rows), f32),
-        pltpu.VMEM((pairs, rows, 2 * rows), f32),
-        pltpu.VMEM((pairs, rows, width), f32),
-        pltpu.VMEM((pairs, rows, width), f32),
-        pltpu.VMEM((pairs, rows, width), f32),
+        pltpu.VMEM((sel_rows, rows), f32),
+        pltpu.VMEM((pairs, 2 * rows, rows), f32),
+        pltpu.VMEM((pairs, 2 * rows, rows), f32),
+        pltpu.VMEM((2 * pairs, rows), f32),
+        pltpu.VMEM((pairs, 2 * sel_rows, rows), bf16),
         pltpu.VMEM((2, 2 * rows, width), f32),
         pltpu.VMEM((2, 2 * rows, width), f32),
         pltpu.VMEM((2, 2 * sel_rows, width), f32),

time: 45.2 us -> 45.4 us (level)
  no operation moved by 1% of the time
where the time goes in v1:
time: 45.4 us; the launch traced here: 45.3 us
  Pallas kernels  40.8 us (90%)
  local copies, waits for them, and re-layouts  3.75 us (8%)
  between operations  0.66 us (1%)
    pallas_call x1, Pallas kernels, per_device_fused(): pl.pallas_call(functools.partial(kernel, n_kv, n_tp), out_shape=(jax.Shap...  40.8 us
    unnamed x10, local copies, waits for them, and re-layouts  3.75 us

profile of v1, /device:TPU:8, one launch (start us, length us, event | category | flops | bytes accessed | tf_op | source)
XLA Modules:
  0.0 45.3 jit_solution(13792691761656533944)
XLA Ops:
  0.6 40.8 %shard_map.102 = (bf16[256,768]{1,0:T(8,128)(2,1)}, bf16[256,128]{1,0:T(8,128)(2,1)}, bf16[256,128]{1,0:T(8,128)(2,1)}, f32[384,128]{1,0:T(8,128)}) custom-call(bf16[256,768]{1,0:T(8,128)(2,1)} %q_hbm.1, bf16[256,128]{1,0:T(8,128)(2,1)} %k_hbm.1, bf16[256,128]{1,0:T(8,128)(2,1)} %v_hbm.1, f32[12,256]{1,0:T(8,128)} %bitcast.1, bf16[256,768]{1,0:T(8,128)(2,1)} %do_hbm.1, ...), custom_call_target="tpu_custom_call" | custom-call | tf_op jit(solution)/shard_map/pallas_call | solution.py:500
  41.5 0.0 copy-start.2
  41.5 0.0 copy-start.1
  41.5 1.8 %copy.15 = bf16[256,768]{1,0:T(8,128)(2,1)} copy(bf16[256,768]{1,0:T(8,128)(2,1)} %get-tuple-element.8) | data formatting | bytes 786432
  43.3 0.0 copy-done.2
  43.3 0.0 copy-start
  43.3 0.6 %copy.16 = bf16[256,128]{1,0:T(8,128)(2,1)} copy(bf16[256,128]{1,0:T(8,128)(2,1)S(1)} %copy-done.2) | data formatting | bytes 131072
  43.9 0.0 copy-done.1
  43.9 0.6 %copy.17 = bf16[256,128]{1,0:T(8,128)(2,1)} copy(bf16[256,128]{1,0:T(8,128)(2,1)S(1)} %copy-done.1) | data formatting | bytes 131072
  44.6 0.0 copy-done
  44.6 0.7 %copy.18 = f32[384,128]{1,0:T(8,128)} copy(f32[384,128]{1,0:T(8,128)S(1)} %copy-done) | data formatting | bytes 393216
Async XLA Ops:
  41.5 1.8 %copy-start.2 = (bf16[256,128]{1,0:T(8,128)(2,1)S(1)}, bf16[256,128]{1,0:T(8,128)(2,1)}, u32[]{:S(2)}) copy-start(bf16[256,128]{1,0:T(8,128)(2,1)} %get-tuple-element.9) | copy-start | bytes 196612
  41.5 2.4 %copy-start.1 = (bf16[256,128]{1,0:T(8,128)(2,1)S(1)}, bf16[256,128]{1,0:T(8,128)(2,1)}, u32[]{:S(2)}) copy-start(bf16[256,128]{1,0:T(8,128)(2,1)} %get-tuple-element.10) | copy-start | bytes 196612
  43.3 1.3 %copy-start = (f32[384,128]{1,0:T(8,128)S(1)}, f32[384,128]{1,0:T(8,128)}, u32[]{:S(2)}) copy-start(f32[384,128]{1,0:T(8,128)} %get-tuple-element.11) | copy-start | bytes 589828

commit v2 on v1

--- a/solution.py
+++ b/solution.py
@@ -12,7 +12,8 @@
 QB = 64
 NSEL = 16
 MASKED = -1e30
-SPREAD_AT = 7
+NEAR_SPREAD = {"ret": (0, 1), ("back", 2): (2,), ("back", 4): (3,)}
+FAR_SPREAD = {("back", 2): (0,), ("back", 4): (1,), "after": (2, 3)}
 MESH = pl.DeviceIdType.MESH
 
 
@@ -40,6 +41,15 @@
     dst[1, rows:] = jnp.where(low, zero, wide).astype(dst.dtype)
 
 
+def xored(index, bits, size):
+    out, bit = index, 1
+    while bit < size:
+        if bits & bit:
+            out = out + bit - 2 * bit * lax.rem(index // bit, 2)
+        bit *= 2
+    return out
+
+
 def turned_keys(pair):
     return jnp.transpose(pair.astype(jnp.float32) * HEAD ** (-0.5)).astype(jnp.bfloat16)
 
@@ -53,12 +63,12 @@
 
 def kernel(
     n_kv, n_tp,
-    q_hbm, k_hbm, v_hbm, lse_hbm, do_hbm, x_ref, chosen_hbm,
+    q_hbm, k_hbm, v_hbm, lse_hbm, do_hbm, x_hbm, chosen_hbm,
     dq_ref, dk_ref, dv_ref, dw_ref,
-    q_ref, do_ref, k_ref, v_ref, lse_ref, chosen_ref, asked, outgoing, fetched, ret_out, ret_in, x_mid, x_all, kg_all,
+    x_ref, q_ref, do_ref, k_ref, v_ref, lse_ref, chosen_ref, asked, outgoing, fetched, ret_out, ret_in, x_mid, x_all, kg_all, half_out, half_in,
     k_own, v_own, k_sel, v_sel, kt_own, kt_sel, bias_own, bias_sel, p_own, dp_own, delta, ds_sel,
     dk_acc, dv_acc, dks_acc, dvs_acc, picks,
-    ask_s, ask_r, blk_s, blk_r, ret_s, ret_r, x1_s, x1_r, x2_s, x2_r, x3_s, xt_s, xt_r, kg_s, kg_r, kgf_s, in_s,
+    ask_s, ask_r, blk_s, blk_r, ret_s, ret_r, x1_s, x1_r, x2_s, x2_r, x3_s, xt_s, xt_r, kg_s, kg_r, half_s, half_r, in_s,
 ):
     me = lax.axis_index("kv")
     col = lax.axis_index("tp")
@@ -72,37 +82,34 @@
     feats = dw_ref.shape[0]
     per_tp = x_ref.shape[1] // feats
     part = rows // n_tp
-    devices = n_kv * n_tp
-    mate = me + 1 - 2 * lax.rem(me, 2)
-    twin = col + 1 - 2 * lax.rem(col, 2)
+    mate = xored(me, 1, n_kv)
+    groups = n_kv // 2
+    group = me // 2
+    lane = lax.rem(me, 2)
+    twin = xored(col, 1, n_tp)
     score_scale = HEAD ** (-0.5)
 
-    loads = [
-        pltpu.make_async_copy(src, dst, in_s.at[n])
-        for n, (src, dst) in enumerate(
+    loads = {
+        name: pltpu.make_async_copy(src, dst, in_s.at[n])
+        for n, (name, src, dst) in enumerate(
             [
-                (chosen_hbm, chosen_ref), (k_hbm, k_ref), (v_hbm, v_ref),
-                (lse_hbm, lse_ref), (q_hbm, q_ref), (do_hbm, do_ref),
+                ("chosen", chosen_hbm, chosen_ref), ("x", x_hbm, x_ref), ("k", k_hbm, k_ref), ("v", v_hbm, v_ref),
+                ("lse", lse_hbm, lse_ref), ("q", q_hbm, q_ref), ("do", do_hbm, do_ref),
             ]
         )
-    ]
-    for load in loads:
+    }
+    for load in loads.values():
         load.start()
+
     asked[...] = jnp.full(asked.shape, -1, jnp.int32)
     fetched[...] = jnp.zeros_like(fetched)
     ret_in[...] = jnp.zeros_like(ret_in)
 
     barrier = pltpu.get_barrier_semaphore()
-    lin = me * n_tp + col
-
-    def greet(d, carry):
-        other = lax.rem(lin + d, devices)
-        pl.semaphore_signal(
-            barrier, inc=1, device_id={"kv": other // n_tp, "tp": lax.rem(other, n_tp)}, device_id_type=MESH
-        )
-        return carry
-
-    lax.fori_loop(1, devices, greet, 0)
+    for d in range(1, n_kv):
+        pl.semaphore_signal(barrier, inc=1, device_id={"kv": lax.rem(me + d, n_kv), "tp": col}, device_id_type=MESH)
+    for d in range(1, n_tp):
+        pl.semaphore_signal(barrier, inc=1, device_id={"kv": me, "tp": lax.rem(col + d, n_tp)}, device_id_type=MESH)
 
     def copy_to(src, dst, s_sem, r_sem, kv=None, tp=None):
         target = {"kv": me if kv is None else kv, "tp": col if tp is None else tp}
@@ -120,88 +127,109 @@
     def return_copy(o):
         return copy_to(ret_out.at[o], ret_in.at[me], ret_s.at[o], ret_r.at[me], kv=o)
 
-    def grad_copy(p):
-        return copy_to(kg_all.at[me], kg_all.at[me], kg_s.at[p], kg_r.at[me], kv=p)
-
-    def forward_grad(p):
-        return copy_to(kg_all.at[p], kg_all.at[p], kgf_s.at[p], kg_r.at[p], kv=mate)
-
-    def quarter(c):
-        return x_all.at[:, pl.ds(pl.multiple_of(c * part, part), part), :]
-
-    def spread_copy(c):
-        return copy_to(quarter(col), quarter(col), x2_s.at[c], x2_r.at[col], tp=c)
-
-    def forward_copy(c):
-        return copy_to(quarter(c), quarter(c), x3_s.at[c], x2_r.at[c], tp=twin)
-
-    def sends_spread(c):
-        return (c != col) & ((lax.rem(c, 2) == lax.rem(col, 2)) | (c == twin))
-
-    def same_core(c):
-        return (c != col) & (lax.rem(c, 2) == lax.rem(col, 2))
-
-    def same_line(p):
-        return (p != me) & (lax.rem(p, 2) == lax.rem(me, 2))
+    def grad_copy(g):
+        return copy_to(kg_all.at[group], kg_all.at[group], kg_s.at[g], kg_r.at[group], kv=2 * g + lane)
+
+    def half_copy():
+        return copy_to(half_out, half_in, half_s, half_r, kv=mate)
+
+    def piece(g, c):
+        return x_all.at[g, pl.ds(pl.multiple_of(c * part, part), part), :]
 
     def cross_copy(c):
         src = x_ref.at[pl.ds(c * part, part), :]
         return copy_to(src, x_mid.at[col], xt_s.at[c], xt_r.at[col], tp=c)
 
-    def line_parts(i):
-        src = x_mid.at[i // per_tp, :, pl.ds((i % per_tp) * feats, feats)]
-        dst = x_all.at[me, pl.ds(pl.multiple_of(col * part, part), part), :]
-        return src, dst
-
-    def line_copy(i):
-        src, dst = line_parts(i)
-        return copy_to(src, dst, x1_s.at[i], x1_r.at[me], kv=i)
-
-    def cross_own(c):
-        return pltpu.make_async_copy(x_ref.at[pl.ds(c * part, part), :], x_mid.at[c], xt_r.at[c])
+    def line_source(g, own):
+        f = pl.ds(((2 * g) % per_tp) * feats, 2 * feats)
+        if own:
+            return x_ref.at[pl.ds(pl.multiple_of(col * part, part), part), f]
+        return x_mid.at[(2 * g) // per_tp, :, f]
+
+    def line_copy(g, own=False):
+        return copy_to(line_source(g, own), piece(group, col), x1_s.at[g], x1_r.at[group], kv=2 * g + lane)
+
+    def start_lines(c, up, own=False):
+        for g in range(groups):
+            if (2 * g) // per_tp != c:
+                continue
+
+            @pl.when(g > group if up else g < group)
+            def _(g=g):
+                line_copy(g, own).start()
+
+            if not up:
+                @pl.when(g == group)
+                def _(g=g):
+                    pltpu.make_async_copy(line_source(g, own), piece(group, col), x1_r.at[g]).start()
 
     def start_cross():
+        for d in (n_tp // 2, n_tp // 2 + 1, 1):
+            for c in range(n_tp):
+                @pl.when(c == xored(col, d, n_tp))
+                def _(c=c):
+                    cross_copy(c).start()
+
+    def own_lines(up):
         for c in range(n_tp):
-            @pl.when(c != col)
-            def _(c=c):
-                cross_copy(c).start()
-
             @pl.when(c == col)
             def _(c=c):
-                cross_own(c).start()
-
-    def start_line():
+                start_lines(c, up, True)
+
+    def lines_of(d, up, wait):
         for c in range(n_tp):
-            @pl.when(c != col)
+            @pl.when(c == xored(col, d, n_tp))
             def _(c=c):
-                copy_to(x_mid.at[c], x_mid.at[c], xt_s.at[c], xt_r.at[c], tp=c).wait_recv()
-
-            @pl.when(c == col)
-            def _(c=c):
-                cross_own(c).wait()
-        for i in range(n_kv):
-            src, dst = line_parts(i)
-
-            @pl.when(i != me)
-            def _(i=i):
-                line_copy(i).start()
-
-            @pl.when(i == me)
-            def _(src=src, dst=dst, i=i):
-                pltpu.make_async_copy(src, dst, x1_r.at[i]).start()
-
-    def start_spread():
-        for p in range(n_kv):
-            piece = x_all.at[p, pl.ds(pl.multiple_of(col * part, part), part), :]
-            pltpu.make_async_copy(piece, piece, x1_r.at[p]).wait()
-        for c in range(n_tp):
-            @pl.when(sends_spread(c))
-            def _(c=c):
-                spread_copy(c).start()
-
-    for load in loads:
-        load.wait()
+                if wait:
+                    copy_to(x_mid.at[c], x_mid.at[c], xt_s.at[c], xt_r.at[c], tp=c).wait_recv()
+                start_lines(c, up)
+
+    across = xored(col, n_tp // 2, n_tp)
+
+    def spread_copy(p, c, k):
+        return copy_to(piece(p, col), piece(p, col), x2_s.at[k, p], x2_r.at[col, p], tp=c)
+
+    def forward_copy(p):
+        return copy_to(piece(p, across), piece(p, across), x3_s.at[p], x2_r.at[across, p], tp=twin)
+
+    def landed_piece(p, c):
+        return copy_to(piece(p, c), piece(p, c), x3_s.at[p], x2_r.at[c, p], tp=twin)
+
+    def spread(d):
+        p = xored(group, d, groups)
+        pltpu.make_async_copy(piece(p, col), piece(p, col), x1_r.at[p]).wait()
+        spread_copy(p, across, 0).start()
+        spread_copy(p, twin, 1).start()
+
+    native = ((2 * group) // per_tp) // (n_tp // 2) == col // (n_tp // 2)
+
+    def spread_at(place):
+        for d in NEAR_SPREAD.get(place, ()):
+            @pl.when(native)
+            def _(d=d):
+                spread(d)
+        for d in FAR_SPREAD.get(place, ()):
+            @pl.when(jnp.logical_not(native))
+            def _(d=d):
+                spread(d)
+
+    early = me >= n_kv // 2
+
+    def meet():
+        pl.semaphore_wait(barrier, n_kv + n_tp - 2)
+        for o in range(n_kv):
+            @pl.when(o < me)
+            def _(o=o):
+                ask_copy(o).start()
+        start_cross()
+        own_lines(True)
+
+    loads["chosen"].wait()
+    loads["x"].wait()
     asked[me, :q_blocks, :NSEL] = chosen_ref[...]
+    pl.when(early)(meet)
+    for name in ("k", "v", "lse", "q", "do"):
+        loads[name].wait()
 
     padded_heads(k_ref[...], k_own, score_scale)
     padded_heads(v_ref[...], v_own, 1.0)
@@ -296,19 +324,10 @@
         else:
             dk_acc[h] += term
 
-    cuts = (pairs // 3, 2 * pairs // 3)
-    for m in range(cuts[0]):
+    for m in range(pairs):
         own_pair(m)
 
-    pl.semaphore_wait(barrier, devices - 1)
-    for o in range(n_kv):
-        @pl.when(o < me)
-        def _(o=o):
-            ask_copy(o).start()
-    start_cross()
-
-    for m in range(cuts[0], cuts[1]):
-        own_pair(m)
+    pl.when(jnp.logical_not(early))(meet)
 
     for p in range(n_kv):
         @pl.when(p > me)
@@ -332,22 +351,22 @@
         def _(p=p):
             block_copy(p).start()
 
-    for m in range(cuts[1], pairs):
-        own_pair(m)
-
-    start_line()
+    own_lines(False)
+    for d in (1, n_tp // 2, n_tp // 2 + 1):
+        lines_of(d, False, True)
     for o in range(n_kv):
         @pl.when(o < me)
         def _(o=o):
             copy_to(fetched.at[o], fetched.at[o], blk_s.at[o], blk_r.at[o], kv=o).wait_recv()
 
+    for d in (1, n_tp // 2, n_tp // 2 + 1):
+        lines_of(d, True, False)
     got = fetched[...].reshape(sel_rows, 2 * width)
     padded_heads(got[:, :width], k_sel, score_scale)
     padded_heads(got[:, width:], v_sel, 1.0)
     kt_sel[...] = turned_keys(got[:, :width])
     for m in range(pairs):
-        if m == SPREAD_AT:
-            start_spread()
+        spread_at(("sel", m))
         sel_pair(m)
 
     ret_out[:, :, :width] = (
@@ -358,13 +377,13 @@
         @pl.when(o < me)
         def _(o=o):
             return_copy(o).start()
-    if SPREAD_AT == pairs:
-        start_spread()
+    spread_at("ret")
     for m in range(pairs):
+        spread_at(("back", m))
         own_pair_back(m)
-    if SPREAD_AT == pairs + 1:
-        start_spread()
-
+    spread_at("after")
+    for d in range(4, groups):
+        spread(d)
     for p in range(n_kv):
         @pl.when(p > me)
         def _(p=p):
@@ -372,46 +391,39 @@
 
     landed = dot_tn(picks[...], ret_in[...].reshape(sel_rows, 2 * width))
     key_grad = (folded_heads(dk_acc, rows) * score_scale + landed[:, :width]).astype(jnp.bfloat16)
-    kg_all[me] = key_grad
-    for p in range(n_kv):
-        @pl.when(same_line(p) | (p == mate))
-        def _(p=p):
-            grad_copy(p).start()
+    kg_all[group] = key_grad
+    for d in (groups // 2, groups // 2 + 1, 1):
+        grad_copy(xored(group, d, groups)).start()
     dk_ref[...] = key_grad
     dv_ref[...] = (folded_heads(dv_acc, rows) + landed[:, width:]).astype(jnp.bfloat16)
 
-    for c in range(n_tp):
-        @pl.when(same_core(c))
-        def _(c=c):
-            copy_to(quarter(c), quarter(c), x2_s.at[c], x2_r.at[c], tp=c).wait_recv()
-            forward_copy(c).start()
-
-    for p in range(n_kv):
-        @pl.when(same_line(p))
-        def _(p=p):
-            copy_to(kg_all.at[p], kg_all.at[p], kg_s.at[p], kg_r.at[p], kv=p).wait_recv()
-            forward_grad(p).start()
-
-    for c in range(n_tp):
-        @pl.when((c != col) & jnp.logical_not(same_core(c)))
-        def _(c=c):
-            copy_to(quarter(c), quarter(c), x2_s.at[c], x2_r.at[c], tp=c).wait_recv()
-
-    total = None
-    for step in range(n_kv // 2):
-        p = lax.rem(me + 2 * step, n_kv)
-        term = dot_tn(x_all[p], kg_all[p])
-        total = term if total is None else total + term
-    dw_ref[...] = total
-    for p in range(n_kv):
-        @pl.when((p != me) & jnp.logical_not(same_line(p)))
-        def _(p=p):
-            copy_to(kg_all.at[p], kg_all.at[p], kg_s.at[p], kg_r.at[p], kv=p).wait_recv()
-    total = dw_ref[...]
-    for step in range(n_kv // 2):
-        p = lax.rem(mate + 2 * step, n_kv)
-        total = total + dot_tn(x_all[p], kg_all[p])
-    dw_ref[...] = total
+    for d in range(groups):
+        p = xored(group, d, groups)
+        landed_piece(p, across).wait_recv()
+        forward_copy(p).start()
+
+    for d in range(1, groups):
+        p = xored(group, d, groups)
+        copy_to(kg_all.at[p], kg_all.at[p], kg_s.at[p], kg_r.at[p], kv=mate).wait_recv()
+
+    for d in range(groups):
+        p = xored(group, d, groups)
+        landed_piece(p, twin).wait_recv()
+        landed_piece(p, xored(twin, n_tp // 2, n_tp)).wait_recv()
+
+    def row_sums(side):
+        at = pl.ds(pl.multiple_of(side * feats, feats), feats)
+        total = None
+        for g in range(groups):
+            term = dot_tn(x_all[g, :, at], kg_all[g])
+            total = term if total is None else total + term
+        return total
+
+    half_out[...] = row_sums(1 - lane).astype(half_out.dtype)
+    half_copy().start()
+    dw_ref[...] = row_sums(lane)
+    half_copy().wait_recv()
+    dw_ref[...] += half_in[...].astype(jnp.float32)
 
     for o in range(n_kv):
         @pl.when(o < me)
@@ -423,32 +435,25 @@
         def _(o=o):
             block_copy(o).wait_send()
 
-        @pl.when(same_line(o) | (o == mate))
-        def _(o=o):
-            grad_copy(o).wait_send()
-
-        @pl.when(same_line(o))
-        def _(o=o):
-            forward_grad(o).wait_send()
-
-    for i in range(n_kv):
-        @pl.when(i != me)
-        def _(i=i):
-            line_copy(i).wait_send()
+    for d in range(1, groups):
+        g = xored(group, d, groups)
+        grad_copy(g).wait_send()
+
+    for g in range(groups):
+        @pl.when(g != group)
+        def _(g=g):
+            line_copy(g).wait_send()
 
     for c in range(n_tp):
         @pl.when(c != col)
         def _(c=c):
             cross_copy(c).wait_send()
 
-    for c in range(n_tp):
-        @pl.when(sends_spread(c))
-        def _(c=c):
-            spread_copy(c).wait_send()
-
-        @pl.when(same_core(c))
-        def _(c=c):
-            forward_copy(c).wait_send()
+    for p in range(groups):
+        spread_copy(p, across, 0).wait_send()
+        spread_copy(p, twin, 1).wait_send()
+        forward_copy(p).wait_send()
+    half_copy().wait_send()
 
 
 def per_device_fused(queries, key_vectors, value_vectors, log_sums, out_grad, layer_input, chosen):
@@ -465,6 +470,7 @@
     vmem = pl.BlockSpec(memory_space=pltpu.VMEM)
     hbm = pl.BlockSpec(memory_space=pl.ANY)
     scratch = [
+        pltpu.VMEM(layer_input.shape, bf16),
         pltpu.VMEM((rows, features), bf16),
         pltpu.VMEM((rows, features), bf16),
         pltpu.VMEM((rows, width), bf16),
@@ -477,8 +483,10 @@
         pltpu.VMEM((n_kv, KB, 2 * width), bf16),
         pltpu.VMEM((n_kv, KB, 2 * width), bf16),
         pltpu.VMEM((n_tp, rows // n_tp, layer_input.shape[1]), bf16),
-        pltpu.VMEM((n_kv, rows, feats), bf16),
-        pltpu.VMEM((n_kv, rows, width), bf16),
+        pltpu.VMEM((n_kv // 2, rows, 2 * feats), bf16),
+        pltpu.VMEM((n_kv // 2, rows, width), bf16),
+        pltpu.VMEM((feats, width), bf16),
+        pltpu.VMEM((feats, width), bf16),
         pltpu.VMEM((2, 2 * rows, width), bf16),
         pltpu.VMEM((2, 2 * rows, width), bf16),
         pltpu.VMEM((2, 2 * sel_rows, width), bf16),
@@ -496,7 +504,7 @@
         pltpu.VMEM((2, 2 * sel_rows, width), f32),
         pltpu.VMEM((2, 2 * sel_rows, width), f32),
         pltpu.VMEM((sel_rows, rows), bf16),
-    ] + [dma((n_kv,))] * 6 + [dma((n_kv,))] * 2 + [dma((n_tp,))] * 5 + [dma((n_kv,))] * 3 + [dma((6,))]
+    ] + [dma((n_kv,))] * 8 + [dma((2, n_kv)), dma((n_tp, n_kv)), dma((n_kv,))] + [dma((n_tp,))] * 2 + [dma((n_kv,))] * 2 + [dma(())] * 2 + [dma((7,))]
     return pl.pallas_call(
         functools.partial(kernel, n_kv, n_tp),
         out_shape=(
@@ -518,8 +526,8 @@
     if (x_features * n_tp) % n_kv or width != 2 * HEAD or features % (6 * width):
         return False
     feats = x_features * n_tp // n_kv
-    whole_tiles = feats % 128 == 0 and x_features % feats == 0 and rows % (16 * n_tp) == 0
-    return whole_tiles and rows // QB <= 8 and n_kv * KB <= 512 and n_kv % 2 == 0 and n_tp % 2 == 0
+    whole_tiles = feats % 128 == 0 and x_features % (2 * feats) == 0 and rows % (16 * n_tp) == 0
+    return whole_tiles and rows // QB <= 8 and n_kv * KB <= 512 and n_kv in (8, 16) and n_tp in (2, 4)
 
 
 def per_device(queries, key_vectors, value_vectors, log_sums, out_grad, layer_input, chosen):

time: 45.4 us -> 39.9 us (0.88)
  the two profiles are of different devices: /device:TPU:8 before, /device:TPU:0 now
where the time goes in v2:
time: 39.9 us; the launch traced here: 39.7 us
  Pallas kernels  35.3 us (88%)
  local copies, waits for them, and re-layouts  3.75 us (9%)
  between operations  0.66 us (2%)
    pallas_call x1, Pallas kernels, per_device_fused(): pl.pallas_call(functools.partial(kernel, n_kv, n_tp), out_shape=(jax.Shap...  35.3 us
    unnamed x10, local copies, waits for them, and re-layouts  3.75 us

profile of v2, /device:TPU:0, one launch (start us, length us, event | category | flops | bytes accessed | tf_op | source)
XLA Modules:
  0.0 39.7 jit_solution(8944738140269828500)
XLA Ops:
  0.6 35.3 %shard_map.102 = (bf16[256,768]{1,0:T(8,128)(2,1)}, bf16[256,128]{1,0:T(8,128)(2,1)}, bf16[256,128]{1,0:T(8,128)(2,1)}, f32[384,128]{1,0:T(8,128)}) custom-call(bf16[256,768]{1,0:T(8,128)(2,1)} %q_hbm.1, bf16[256,128]{1,0:T(8,128)(2,1)} %k_hbm.1, bf16[256,128]{1,0:T(8,128)(2,1)} %v_hbm.1, f32[12,256]{1,0:T(8,128)} %bitcast.1, bf16[256,768]{1,0:T(8,128)(2,1)} %do_hbm.1, ...), custom_call_target="tpu_custom_call" | custom-call | tf_op jit(solution)/shard_map/pallas_call | solution.py:508
  35.9 0.0 copy-start.2
  36.0 0.0 copy-start.1
  36.0 1.8 %copy.15 = bf16[256,768]{1,0:T(8,128)(2,1)} copy(bf16[256,768]{1,0:T(8,128)(2,1)} %get-tuple-element.8) | data formatting | bytes 786432
  37.8 0.0 copy-done.2
  37.8 0.0 copy-start
  37.8 0.6 %copy.16 = bf16[256,128]{1,0:T(8,128)(2,1)} copy(bf16[256,128]{1,0:T(8,128)(2,1)S(1)} %copy-done.2) | data formatting | bytes 131072
  38.4 0.0 copy-done.1
  38.4 0.6 %copy.17 = bf16[256,128]{1,0:T(8,128)(2,1)} copy(bf16[256,128]{1,0:T(8,128)(2,1)S(1)} %copy-done.1) | data formatting | bytes 131072
  39.0 0.0 copy-done
  39.0 0.7 %copy.18 = f32[384,128]{1,0:T(8,128)} copy(f32[384,128]{1,0:T(8,128)S(1)} %copy-done) | data formatting | bytes 393216
Async XLA Ops:
  35.9 1.8 %copy-start.2 = (bf16[256,128]{1,0:T(8,128)(2,1)S(1)}, bf16[256,128]{1,0:T(8,128)(2,1)}, u32[]{:S(2)}) copy-start(bf16[256,128]{1,0:T(8,128)(2,1)} %get-tuple-element.9) | copy-start | bytes 196612
  36.0 2.4 %copy-start.1 = (bf16[256,128]{1,0:T(8,128)(2,1)S(1)}, bf16[256,128]{1,0:T(8,128)(2,1)}, u32[]{:S(2)}) copy-start(bf16[256,128]{1,0:T(8,128)(2,1)} %get-tuple-element.10) | copy-start | bytes 196612
  37.8 1.3 %copy-start = (f32[384,128]{1,0:T(8,128)S(1)}, f32[384,128]{1,0:T(8,128)}, u32[]{:S(2)}) copy-start(f32[384,128]{1,0:T(8,128)} %get-tuple-element.11) | copy-start | bytes 589828

commit v3 on v2

--- a/solution.py
+++ b/solution.py
@@ -12,8 +12,6 @@
 QB = 64
 NSEL = 16
 MASKED = -1e30
-NEAR_SPREAD = {"ret": (0, 1), ("back", 2): (2,), ("back", 4): (3,)}
-FAR_SPREAD = {("back", 2): (0,), ("back", 4): (1,), "after": (2, 3)}
 MESH = pl.DeviceIdType.MESH
 
 
@@ -65,40 +63,47 @@
     n_kv, n_tp,
     q_hbm, k_hbm, v_hbm, lse_hbm, do_hbm, x_hbm, chosen_hbm,
     dq_ref, dk_ref, dv_ref, dw_ref,
-    x_ref, q_ref, do_ref, k_ref, v_ref, lse_ref, chosen_ref, asked, outgoing, fetched, ret_out, ret_in, x_mid, x_all, kg_all, half_out, half_in,
+    x_ref, qd_ref, kv_ref, lse_ref, chosen_ref, asked, outgoing, fetched, ret_out, ret_in, x_all, x_t, kg_all, half_out, half_in, half_sum,
     k_own, v_own, k_sel, v_sel, kt_own, kt_sel, bias_own, bias_sel, p_own, dp_own, delta, ds_sel,
-    dk_acc, dv_acc, dks_acc, dvs_acc, picks,
-    ask_s, ask_r, blk_s, blk_r, ret_s, ret_r, x1_s, x1_r, x2_s, x2_r, x3_s, xt_s, xt_r, kg_s, kg_r, half_s, half_r, in_s,
+    dk_acc, dv_acc, dks_acc, dvs_acc, picks, picks_t,
+    ask_s, ask_r, blk_s, blk_r, ret_r, x1_s, x1_r, x2_r, x3_r, xs_s, xf_s, kg_s, kg_r, half_s, half_r, in_s,
 ):
     me = lax.axis_index("kv")
     col = lax.axis_index("tp")
-    rows = q_ref.shape[0]
-    width = k_ref.shape[1]
-    pairs = q_ref.shape[1] // width
+    rows = qd_ref.shape[1]
+    width = kv_ref.shape[2]
+    pairs = qd_ref.shape[2] // width
     per_head = pairs // 2
     here = rows // KB
     q_blocks = rows // QB
     sel_rows = n_kv * KB
     feats = dw_ref.shape[0]
     per_tp = x_ref.shape[1] // feats
-    part = rows // n_tp
-    mate = xored(me, 1, n_kv)
-    groups = n_kv // 2
-    group = me // 2
-    lane = lax.rem(me, 2)
+    mate = xored(me, n_kv // 2, n_kv)
+    half = n_kv // 2
+    cores = n_tp // 2
+    slot = lax.rem(me, half)
+    first = me - slot
+    part_of = me // half
+    side = col // cores
+    native = lax.rem(me // per_tp, cores) == lax.rem(col, cores)
     twin = xored(col, 1, n_tp)
     score_scale = HEAD ** (-0.5)
 
-    loads = {
-        name: pltpu.make_async_copy(src, dst, in_s.at[n])
-        for n, (name, src, dst) in enumerate(
-            [
-                ("chosen", chosen_hbm, chosen_ref), ("x", x_hbm, x_ref), ("k", k_hbm, k_ref), ("v", v_hbm, v_ref),
-                ("lse", lse_hbm, lse_ref), ("q", q_hbm, q_ref), ("do", do_hbm, do_ref),
-            ]
-        )
-    }
-    for load in loads.values():
+    loads = [
+        pltpu.make_async_copy(src, dst, sem)
+        for src, dst, sem in [
+            (chosen_hbm, chosen_ref, in_s.at[0]), (x_hbm, x_ref, in_s.at[1]),
+            (k_hbm, kv_ref.at[0], in_s.at[2]), (v_hbm, kv_ref.at[1], in_s.at[2]), (lse_hbm, lse_ref, in_s.at[3]),
+            (q_hbm, qd_ref.at[0], in_s.at[4]), (do_hbm, qd_ref.at[1], in_s.at[4]),
+        ]
+    ]
+    k_ref, v_ref, q_ref, do_ref = kv_ref.at[0], kv_ref.at[1], qd_ref.at[0], qd_ref.at[1]
+
+    def wait_for(ref, sem):
+        pltpu.make_async_copy(ref, ref, sem).wait()
+
+    for load in loads:
         load.start()
 
     asked[...] = jnp.full(asked.shape, -1, jnp.int32)
@@ -119,99 +124,55 @@
         )
 
     def ask_copy(o):
-        return copy_to(asked.at[me], asked.at[me], ask_s.at[o], ask_r.at[me], kv=o)
+        return copy_to(asked.at[me], asked.at[me], ask_s, ask_r, kv=o)
 
     def block_copy(p):
-        return copy_to(outgoing.at[p], fetched.at[me], blk_s.at[p], blk_r.at[me], kv=p)
+        return copy_to(outgoing.at[p], fetched.at[me], blk_s, blk_r, kv=p)
 
     def return_copy(o):
-        return copy_to(ret_out.at[o], ret_in.at[me], ret_s.at[o], ret_r.at[me], kv=o)
+        return copy_to(ret_out.at[o], ret_in.at[me], blk_s, ret_r, kv=o)
 
     def grad_copy(g):
-        return copy_to(kg_all.at[group], kg_all.at[group], kg_s.at[g], kg_r.at[group], kv=2 * g + lane)
+        return copy_to(kg_all.at[slot], kg_all.at[slot], kg_s, kg_r.at[slot], kv=first + g)
 
     def half_copy():
         return copy_to(half_out, half_in, half_s, half_r, kv=mate)
 
-    def piece(g, c):
-        return x_all.at[g, pl.ds(pl.multiple_of(c * part, part), part), :]
-
-    def cross_copy(c):
-        src = x_ref.at[pl.ds(c * part, part), :]
-        return copy_to(src, x_mid.at[col], xt_s.at[c], xt_r.at[col], tp=c)
-
-    def line_source(g, own):
-        f = pl.ds(((2 * g) % per_tp) * feats, 2 * feats)
-        if own:
-            return x_ref.at[pl.ds(pl.multiple_of(col * part, part), part), f]
-        return x_mid.at[(2 * g) // per_tp, :, f]
-
-    def line_copy(g, own=False):
-        return copy_to(line_source(g, own), piece(group, col), x1_s.at[g], x1_r.at[group], kv=2 * g + lane)
-
-    def start_lines(c, up, own=False):
-        for g in range(groups):
-            if (2 * g) // per_tp != c:
-                continue
-
-            @pl.when(g > group if up else g < group)
-            def _(g=g):
-                line_copy(g, own).start()
-
-            if not up:
-                @pl.when(g == group)
-                def _(g=g):
-                    pltpu.make_async_copy(line_source(g, own), piece(group, col), x1_r.at[g]).start()
-
-    def start_cross():
-        for d in (n_tp // 2, n_tp // 2 + 1, 1):
-            for c in range(n_tp):
-                @pl.when(c == xored(col, d, n_tp))
-                def _(c=c):
-                    cross_copy(c).start()
-
-    def own_lines(up):
-        for c in range(n_tp):
-            @pl.when(c == col)
-            def _(c=c):
-                start_lines(c, up, True)
-
-    def lines_of(d, up, wait):
-        for c in range(n_tp):
-            @pl.when(c == xored(col, d, n_tp))
-            def _(c=c):
-                if wait:
-                    copy_to(x_mid.at[c], x_mid.at[c], xt_s.at[c], xt_r.at[c], tp=c).wait_recv()
-                start_lines(c, up)
-
-    across = xored(col, n_tp // 2, n_tp)
-
-    def spread_copy(p, c, k):
-        return copy_to(piece(p, col), piece(p, col), x2_s.at[k, p], x2_r.at[col, p], tp=c)
-
-    def forward_copy(p):
-        return copy_to(piece(p, across), piece(p, across), x3_s.at[p], x2_r.at[across, p], tp=twin)
-
-    def landed_piece(p, c):
-        return copy_to(piece(p, c), piece(p, c), x3_s.at[p], x2_r.at[c, p], tp=twin)
+    def line_source(j):
+        return x_ref.at[:, pl.ds((j % per_tp) * feats, feats)]
+
+    def start_lines():
+        for j in range(half):
+            mine = (j // per_tp) % cores == lax.rem(col, cores)
+
+            @pl.when(mine & (j != slot))
+            def _(j=j):
+                copy_to(line_source(j), x_all.at[side, slot], x1_s, x1_r.at[slot], kv=first + j).start()
+
+            @pl.when(mine & (j == slot))
+            def _(j=j):
+                pltpu.make_async_copy(line_source(j), x_all.at[side, slot], x1_r.at[j]).start()
+
+    per_core = half // cores
+    line_count = jnp.where(native, per_core - 1, per_core)
+    across = xored(col, cores, n_tp)
 
     def spread(d):
-        p = xored(group, d, groups)
-        pltpu.make_async_copy(piece(p, col), piece(p, col), x1_r.at[p]).wait()
-        spread_copy(p, across, 0).start()
-        spread_copy(p, twin, 1).start()
-
-    native = ((2 * group) // per_tp) // (n_tp // 2) == col // (n_tp // 2)
-
-    def spread_at(place):
-        for d in NEAR_SPREAD.get(place, ()):
-            @pl.when(native)
-            def _(d=d):
-                spread(d)
-        for d in FAR_SPREAD.get(place, ()):
-            @pl.when(jnp.logical_not(native))
-            def _(d=d):
-                spread(d)
+        p = xored(slot, d, half)
+
+        @pl.when(native)
+        def _():
+            wait_for(x_all.at[side, p], x1_r.at[p])
+            copy_to(x_all.at[side, p], x_all.at[side, p], xs_s, x2_r.at[p], tp=across).start()
+            copy_to(x_all.at[side, p], x_all.at[side, p], xf_s, x3_r, tp=twin).start()
+
+    def forward(d):
+        p = xored(slot, d, half)
+
+        @pl.when(native)
+        def _():
+            wait_for(x_all.at[1 - side, p], x2_r.at[p])
+            copy_to(x_all.at[1 - side, p], x_all.at[1 - side, p], xf_s, x3_r, tp=twin).start()
 
     early = me >= n_kv // 2
 
@@ -221,15 +182,16 @@
             @pl.when(o < me)
             def _(o=o):
                 ask_copy(o).start()
-        start_cross()
-        own_lines(True)
-
-    loads["chosen"].wait()
-    loads["x"].wait()
+        start_lines()
+        spread(0)
+
+    loads[0].wait()
+    loads[1].wait()
     asked[me, :q_blocks, :NSEL] = chosen_ref[...]
     pl.when(early)(meet)
-    for name in ("k", "v", "lse", "q", "do"):
-        loads[name].wait()
+    wait_for(kv_ref, in_s.at[2])
+    loads[4].wait()
+    wait_for(qd_ref, in_s.at[4])
 
     padded_heads(k_ref[...], k_own, score_scale)
     padded_heads(v_ref[...], v_own, 1.0)
@@ -329,10 +291,10 @@
 
     pl.when(jnp.logical_not(early))(meet)
 
-    for p in range(n_kv):
-        @pl.when(p > me)
-        def _(p=p):
-            copy_to(asked.at[p], asked.at[p], ask_s.at[p], ask_r.at[p], kv=p).wait_recv()
+    for r in range(n_kv - 1):
+        @pl.when(me == r)
+        def _(r=r):
+            wait_for(asked.at[pl.ds(r + 1, n_kv - 1 - r)], ask_r)
 
     wants = asked[...]
     mine = (wants >= me * here) & (wants < me * here + here)
@@ -351,22 +313,19 @@
         def _(p=p):
             block_copy(p).start()
 
-    own_lines(False)
-    for d in (1, n_tp // 2, n_tp // 2 + 1):
-        lines_of(d, False, True)
-    for o in range(n_kv):
-        @pl.when(o < me)
-        def _(o=o):
-            copy_to(fetched.at[o], fetched.at[o], blk_s.at[o], blk_r.at[o], kv=o).wait_recv()
-
-    for d in (1, n_tp // 2, n_tp // 2 + 1):
-        lines_of(d, True, False)
+    for d in range(1, half):
+        spread(d)
+    picks_t[...] = jnp.transpose(picks[...])
+    for r in range(1, n_kv):
+        @pl.when(me == r)
+        def _(r=r):
+            wait_for(fetched.at[pl.ds(0, r)], blk_r)
+
     got = fetched[...].reshape(sel_rows, 2 * width)
     padded_heads(got[:, :width], k_sel, score_scale)
     padded_heads(got[:, width:], v_sel, 1.0)
     kt_sel[...] = turned_keys(got[:, :width])
     for m in range(pairs):
-        spread_at(("sel", m))
         sel_pair(m)
 
     ret_out[:, :, :width] = (
@@ -377,83 +336,79 @@
         @pl.when(o < me)
         def _(o=o):
             return_copy(o).start()
-    spread_at("ret")
     for m in range(pairs):
-        spread_at(("back", m))
         own_pair_back(m)
-    spread_at("after")
-    for d in range(4, groups):
-        spread(d)
-    for p in range(n_kv):
-        @pl.when(p > me)
-        def _(p=p):
-            copy_to(ret_in.at[p], ret_in.at[p], ret_s.at[p], ret_r.at[p], kv=p).wait_recv()
-
-    landed = dot_tn(picks[...], ret_in[...].reshape(sel_rows, 2 * width))
+    for d in range(half):
+        forward(d)
+
+    @pl.when(jnp.logical_not(native))
+    def _():
+        wait_for(x_all, x3_r)
+
+    for s in range(2):
+        for g in range(half):
+            x_t[s, g] = jnp.transpose(x_all[s, g])
+
+    for r in range(n_kv - 1):
+        @pl.when(me == r)
+        def _(r=r):
+            wait_for(ret_in.at[pl.ds(r + 1, n_kv - 1 - r)], ret_r)
+
+    landed = dot_nn(picks_t[...], ret_in[...].reshape(sel_rows, 2 * width))
     key_grad = (folded_heads(dk_acc, rows) * score_scale + landed[:, :width]).astype(jnp.bfloat16)
-    kg_all[group] = key_grad
-    for d in (groups // 2, groups // 2 + 1, 1):
-        grad_copy(xored(group, d, groups)).start()
+    kg_all[slot] = key_grad
+    for d in range(half - 1, 0, -1):
+        grad_copy(xored(slot, d, half)).start()
     dk_ref[...] = key_grad
     dv_ref[...] = (folded_heads(dv_acc, rows) + landed[:, width:]).astype(jnp.bfloat16)
 
-    for d in range(groups):
-        p = xored(group, d, groups)
-        landed_piece(p, across).wait_recv()
-        forward_copy(p).start()
-
-    for d in range(1, groups):
-        p = xored(group, d, groups)
-        copy_to(kg_all.at[p], kg_all.at[p], kg_s.at[p], kg_r.at[p], kv=mate).wait_recv()
-
-    for d in range(groups):
-        p = xored(group, d, groups)
-        landed_piece(p, twin).wait_recv()
-        landed_piece(p, xored(twin, n_tp // 2, n_tp)).wait_recv()
-
-    def row_sums(side):
-        at = pl.ds(pl.multiple_of(side * feats, feats), feats)
-        total = None
-        for g in range(groups):
-            term = dot_tn(x_all[g, :, at], kg_all[g])
-            total = term if total is None else total + term
-        return total
-
-    half_out[...] = row_sums(1 - lane).astype(half_out.dtype)
+    def row_sums(d, s):
+        p = xored(slot, d, half)
+        return dot_nn(x_t[s, p], kg_all[p])
+
+    theirs, ours = row_sums(0, 1 - part_of), row_sums(0, part_of)
+    half_sum[...] = theirs
+    dw_ref[...] = ours
+    for d in range(1, half):
+        g = xored(slot, d, half)
+        wait_for(kg_all.at[g], kg_r.at[g])
+        if d < half - 1:
+            half_sum[...] += row_sums(d, 1 - part_of)
+            dw_ref[...] += row_sums(d, part_of)
+    half_out[...] = (half_sum[...] + row_sums(half - 1, 1 - part_of)).astype(half_out.dtype)
     half_copy().start()
-    dw_ref[...] = row_sums(lane)
+    dw_ref[...] += row_sums(half - 1, part_of)
     half_copy().wait_recv()
     dw_ref[...] += half_in[...].astype(jnp.float32)
 
-    for o in range(n_kv):
-        @pl.when(o < me)
-        def _(o=o):
-            ask_copy(o).wait_send()
-            return_copy(o).wait_send()
-
-        @pl.when(o > me)
-        def _(o=o):
-            block_copy(o).wait_send()
-
-    for d in range(1, groups):
-        g = xored(group, d, groups)
-        grad_copy(g).wait_send()
-
-    for g in range(groups):
-        @pl.when(g != group)
-        def _(g=g):
-            line_copy(g).wait_send()
-
-    for c in range(n_tp):
-        @pl.when(c != col)
-        def _(c=c):
-            cross_copy(c).wait_send()
-
-    for p in range(groups):
-        spread_copy(p, across, 0).wait_send()
-        spread_copy(p, twin, 1).wait_send()
-        forward_copy(p).wait_send()
+    for r in range(1, n_kv):
+        @pl.when(me == r)
+        def _(r=r):
+            wait_for(asked.at[pl.ds(0, r)], ask_s)
+    wait_for(fetched.at[pl.ds(0, n_kv - 1)], blk_s)
+    wait_for(kg_all.at[pl.ds(0, half - 1)], kg_s)
+    for count in range(1, half + 1):
+        @pl.when(line_count == count)
+        def _(count=count):
+            wait_for(x_all.at[0, pl.ds(0, count)], x1_s)
+
+    @pl.when(native)
+    def _():
+        wait_for(x_all.at[0], xs_s)
+        wait_for(x_all, xf_s)
+
     half_copy().wait_send()
+
+
+def put_out(a, b, c, d, a_out, b_out, c_out, d_out, sems):
+    copies = [
+        pltpu.make_async_copy(src, dst, sems.at[n])
+        for n, (src, dst) in enumerate([(a, a_out), (b, b_out), (c, c_out), (d, d_out)])
+    ]
+    for copy in copies:
+        copy.start()
+    for copy in copies:
+        copy.wait()
 
 
 def per_device_fused(queries, key_vectors, value_vectors, log_sums, out_grad, layer_input, chosen):
@@ -471,10 +426,8 @@
     hbm = pl.BlockSpec(memory_space=pl.ANY)
     scratch = [
         pltpu.VMEM(layer_input.shape, bf16),
-        pltpu.VMEM((rows, features), bf16),
-        pltpu.VMEM((rows, features), bf16),
-        pltpu.VMEM((rows, width), bf16),
-        pltpu.VMEM((rows, width), bf16),
+        pltpu.VMEM((2, rows, features), bf16),
+        pltpu.VMEM((2, rows, width), bf16),
         pltpu.VMEM((log_sums.shape[1], rows), f32),
         pltpu.VMEM(chosen.shape, jnp.int32),
         pltpu.VMEM((n_kv, 8, 128), jnp.int32),
@@ -482,11 +435,12 @@
         pltpu.VMEM((n_kv, KB, 2 * width), bf16),
         pltpu.VMEM((n_kv, KB, 2 * width), bf16),
         pltpu.VMEM((n_kv, KB, 2 * width), bf16),
-        pltpu.VMEM((n_tp, rows // n_tp, layer_input.shape[1]), bf16),
-        pltpu.VMEM((n_kv // 2, rows, 2 * feats), bf16),
+        pltpu.VMEM((2, n_kv // 2, rows, feats), bf16),
+        pltpu.VMEM((2, n_kv // 2, feats, rows), bf16),
         pltpu.VMEM((n_kv // 2, rows, width), bf16),
         pltpu.VMEM((feats, width), bf16),
         pltpu.VMEM((feats, width), bf16),
+        pltpu.VMEM((feats, width), f32),
         pltpu.VMEM((2, 2 * rows, width), bf16),
         pltpu.VMEM((2, 2 * rows, width), bf16),
         pltpu.VMEM((2, 2 * sel_rows, width), bf16),
@@ -504,30 +458,43 @@
         pltpu.VMEM((2, 2 * sel_rows, width), f32),
         pltpu.VMEM((2, 2 * sel_rows, width), f32),
         pltpu.VMEM((sel_rows, rows), bf16),
-    ] + [dma((n_kv,))] * 8 + [dma((2, n_kv)), dma((n_tp, n_kv)), dma((n_kv,))] + [dma((n_tp,))] * 2 + [dma((n_kv,))] * 2 + [dma(())] * 2 + [dma((7,))]
-    return pl.pallas_call(
+        pltpu.VMEM((rows, sel_rows), bf16),
+    ] + [
+        dma(()), dma(()), dma(()), dma(()), dma(()), dma(()), dma((n_kv // 2,)), dma((n_kv // 2,)), dma(()), dma(()),
+        dma(()), dma(()), dma((n_kv // 2,)), dma(()), dma(()), dma((5,)),
+    ]
+    shapes = (((rows, features), bf16), ((rows, width), bf16), ((rows, width), bf16), ((feats, width), f32))
+    held = pl.pallas_call(
         functools.partial(kernel, n_kv, n_tp),
-        out_shape=(
-            jax.ShapeDtypeStruct((rows, features), bf16),
-            jax.ShapeDtypeStruct((rows, width), bf16),
-            jax.ShapeDtypeStruct((rows, width), bf16),
-            jax.ShapeDtypeStruct((feats, width), f32),
-        ),
+        out_shape=tuple(pltpu.VMEM(shape, dtype) for shape, dtype in shapes),
         in_specs=[hbm] * 7,
         out_specs=(vmem,) * 4,
         scratch_shapes=scratch,
         compiler_params=pltpu.CompilerParams(
-            collective_id=0, has_side_effects=True
+            collective_id=0, has_side_effects=True, vmem_limit_bytes=40 << 20
         ),
-    )(queries, key_vectors, value_vectors, log_sums.T, out_grad, layer_input, chosen)
+    )(
+        *(
+            pltpu.with_memory_space_constraint(x, pltpu.HBM)
+            for x in (queries, key_vectors, value_vectors, log_sums.T, out_grad, layer_input, chosen)
+        )
+    )
+    return pl.pallas_call(
+        put_out,
+        out_shape=tuple(jax.ShapeDtypeStruct(shape, dtype) for shape, dtype in shapes),
+        in_specs=[vmem] * 4,
+        out_specs=(hbm,) * 4,
+        scratch_shapes=[dma((4,))],
+        compiler_params=pltpu.CompilerParams(vmem_limit_bytes=8 << 20),
+    )(*(pltpu.with_memory_space_constraint(x, pltpu.VMEM) for x in held))
 
 
 def fits_fused(n_kv, n_tp, rows, features, width, x_features):
     if (x_features * n_tp) % n_kv or width != 2 * HEAD or features % (6 * width):
         return False
     feats = x_features * n_tp // n_kv
-    whole_tiles = feats % 128 == 0 and x_features % (2 * feats) == 0 and rows % (16 * n_tp) == 0
-    return whole_tiles and rows // QB <= 8 and n_kv * KB <= 512 and n_kv in (8, 16) and n_tp in (2, 4)
+    whole_tiles = feats % 128 == 0 and x_features % feats == 0 and n_kv % n_tp == 0 and rows % 16 == 0
+    return whole_tiles and rows // QB <= 8 and n_kv * KB <= 512 and n_kv in (8, 16) and n_tp == 4
 
 
 def per_device(queries, key_vectors, value_vectors, log_sums, out_grad, layer_input, chosen):

time: 39.9 us -> 33.6 us (0.84)
  the two profiles are of different devices: /device:TPU:0 before, /device:TPU:4 now
where the time goes in v3:
time: 33.6 us; the launch traced here: 33.4 us
  Pallas kernels  32.8 us (98%)
  between operations  0.64 us (2%)
    pallas_call x1, Pallas kernels, per_device_fused(): pl.pallas_call(functools.partial(kernel, n_kv, n_tp), out_shape=tuple((pl...  31.9 us
    pallas_call x1, Pallas kernels, per_device_fused(): pl.pallas_call(put_out, out_shape=tuple((jax.ShapeDtypeStruct(shape, dtyp...  0.89 us

profile of v3, /device:TPU:4, one launch (start us, length us, event | category | flops | bytes accessed | tf_op | source)
XLA Modules:
  0.0 33.4 jit_solution(2807849445701110888)
XLA Ops:
  0.6 31.9 %shard_map.102 = (bf16[256,768]{1,0:T(8,128)(2,1)S(1)}, bf16[256,128]{1,0:T(8,128)(2,1)S(1)}, bf16[256,128]{1,0:T(8,128)(2,1)S(1)}, f32[384,128]{1,0:T(8,128)S(1)}) custom-call(bf16[256,768]{1,0:T(8,128)(2,1)} %q_hbm.1, bf16[256,128]{1,0:T(8,128)(2,1)} %k_hbm.1, bf16[256,128]{1,0:T(8,128)(2,1)} %v_hbm.1, f32[12,256]{1,0:T(8,128)} %bitcast.1, ...), custom_call_target="tpu_custom_call" | custom-call | tf_op jit(solution)/shard_map/pallas_call | solution.py:467
  32.5 0.9 %shard_map.103 = (bf16[256,768]{1,0:T(8,128)(2,1)}, bf16[256,128]{1,0:T(8,128)(2,1)}, bf16[256,128]{1,0:T(8,128)(2,1)}, f32[384,128]{1,0:T(8,128)}) custom-call(bf16[256,768]{1,0:T(8,128)(2,1)S(1)} %get-tuple-element.8.a, bf16[256,128]{1,0:T(8,128)(2,1)S(1)} %get-tuple-element.9.b, bf16[256,128]{1,0:T(8,128)(2,1)S(1)} %get-tuple-element.10.c, ...), custom_call_target="tpu_custom_call" | custom-call | tf_op jit(solution)/shard_map/pallas_call | solution.py:482

commit v4 on v3

--- a/solution.py
+++ b/solution.py
@@ -63,7 +63,7 @@
     n_kv, n_tp,
     q_hbm, k_hbm, v_hbm, lse_hbm, do_hbm, x_hbm, chosen_hbm,
     dq_ref, dk_ref, dv_ref, dw_ref,
-    x_ref, qd_ref, kv_ref, lse_ref, chosen_ref, asked, outgoing, fetched, ret_out, ret_in, x_all, x_t, kg_all, half_out, half_in, half_sum,
+    x_ref, qd_ref, kv_ref, lse_ref, chosen_ref, asking, asked, outgoing, fetched, ret_out, ret_in, x_all, x_t, kg_all, half_out, half_in, half_sum,
     k_own, v_own, k_sel, v_sel, kt_own, kt_sel, bias_own, bias_sel, p_own, dp_own, delta, ds_sel,
     dk_acc, dv_acc, dks_acc, dvs_acc, picks, picks_t,
     ask_s, ask_r, blk_s, blk_r, ret_r, x1_s, x1_r, x2_r, x3_r, xs_s, xf_s, kg_s, kg_r, half_s, half_r, in_s,
@@ -111,8 +111,10 @@
     ret_in[...] = jnp.zeros_like(ret_in)
 
     barrier = pltpu.get_barrier_semaphore()
-    for d in range(1, n_kv):
-        pl.semaphore_signal(barrier, inc=1, device_id={"kv": lax.rem(me + d, n_kv), "tp": col}, device_id_type=MESH)
+    for p in range(n_kv):
+        @pl.when((p > me) | ((p // half == part_of) & (p != me)))
+        def _(p=p):
+            pl.semaphore_signal(barrier, inc=1, device_id={"kv": p, "tp": col}, device_id_type=MESH)
     for d in range(1, n_tp):
         pl.semaphore_signal(barrier, inc=1, device_id={"kv": me, "tp": lax.rem(col + d, n_tp)}, device_id_type=MESH)
 
@@ -124,7 +126,7 @@
         )
 
     def ask_copy(o):
-        return copy_to(asked.at[me], asked.at[me], ask_s, ask_r, kv=o)
+        return copy_to(asking.at[o], asked.at[me], ask_s, ask_r, kv=o)
 
     def block_copy(p):
         return copy_to(outgoing.at[p], fetched.at[me], blk_s, blk_r, kv=p)
@@ -174,21 +176,20 @@
             wait_for(x_all.at[1 - side, p], x2_r.at[p])
             copy_to(x_all.at[1 - side, p], x_all.at[1 - side, p], xf_s, x3_r, tp=twin).start()
 
-    early = me >= n_kv // 2
-
-    def meet():
-        pl.semaphore_wait(barrier, n_kv + n_tp - 2)
-        for o in range(n_kv):
-            @pl.when(o < me)
-            def _(o=o):
-                ask_copy(o).start()
-        start_lines()
-        spread(0)
-
     loads[0].wait()
+    owner_rows = lax.broadcasted_iota(jnp.int32, (n_kv, q_blocks, NSEL), 0) * here
+    entries = chosen_ref[...][None] - owner_rows
+    wanted = jnp.where((entries >= 0) & (entries < here), entries, -1)
+    wanted = jnp.max(jnp.max(wanted, axis=2, keepdims=True), axis=1, keepdims=True)
+    asking[...] = jnp.broadcast_to(wanted, asking.shape)
+    pl.semaphore_wait(barrier, first + half - 1 + n_tp - 1)
+    for o in range(n_kv):
+        @pl.when(o < me)
+        def _(o=o):
+            ask_copy(o).start()
     loads[1].wait()
-    asked[me, :q_blocks, :NSEL] = chosen_ref[...]
-    pl.when(early)(meet)
+    start_lines()
+    spread(0)
     wait_for(kv_ref, in_s.at[2])
     loads[4].wait()
     wait_for(qd_ref, in_s.at[4])
@@ -289,26 +290,20 @@
     for m in range(pairs):
         own_pair(m)
 
-    pl.when(jnp.logical_not(early))(meet)
-
     for r in range(n_kv - 1):
         @pl.when(me == r)
         def _(r=r):
             wait_for(asked.at[pl.ds(r + 1, n_kv - 1 - r)], ask_r)
 
-    wants = asked[...]
-    mine = (wants >= me * here) & (wants < me * here + here)
-    local = jnp.where(mine, wants - me * here, -1)
-    local = jnp.max(jnp.max(local, axis=2, keepdims=True), axis=1, keepdims=True)
     shape = (n_kv, KB, rows)
-    at = lax.broadcasted_iota(jnp.int32, shape, 2)
-    offset = lax.broadcasted_iota(jnp.int32, shape, 1)
+    at = lax.broadcasted_iota(jnp.int32, shape, 2) - lax.broadcasted_iota(jnp.int32, shape, 1)
     sender = lax.broadcasted_iota(jnp.int32, shape, 0)
-    chosen_here = (local >= 0) & (sender > me) & (at == local * KB + offset)
+    local = jnp.concatenate([jnp.concatenate([asked[...]] * (KB // 8), axis=1)] * (rows // 128), axis=2)
+    chosen_here = (local >= 0) & (sender > me) & (at == local * KB)
     picks[...] = jnp.where(chosen_here, 1.0, 0.0).astype(jnp.bfloat16).reshape(sel_rows, rows)
-    outgoing[:, :, :width] = dot_nn(picks[...], k_ref[...]).astype(jnp.bfloat16).reshape(n_kv, KB, width)
-    outgoing[:, :, width:] = dot_nn(picks[...], v_ref[...]).astype(jnp.bfloat16).reshape(n_kv, KB, width)
-    for p in range(n_kv):
+    both = jnp.concatenate([k_ref[...], v_ref[...]], axis=1)
+    outgoing[...] = dot_nn(picks[...], both).astype(jnp.bfloat16).reshape(n_kv, KB, 2 * width)
+    for p in reversed(range(n_kv)):
         @pl.when(p > me)
         def _(p=p):
             block_copy(p).start()
@@ -332,23 +327,12 @@
         (folded_heads(dks_acc, sel_rows) * score_scale).astype(ret_out.dtype).reshape(n_kv, KB, width)
     )
     ret_out[:, :, width:] = folded_heads(dvs_acc, sel_rows).astype(ret_out.dtype).reshape(n_kv, KB, width)
-    for o in range(n_kv):
+    for o in reversed(range(n_kv)):
         @pl.when(o < me)
         def _(o=o):
             return_copy(o).start()
     for m in range(pairs):
         own_pair_back(m)
-    for d in range(half):
-        forward(d)
-
-    @pl.when(jnp.logical_not(native))
-    def _():
-        wait_for(x_all, x3_r)
-
-    for s in range(2):
-        for g in range(half):
-            x_t[s, g] = jnp.transpose(x_all[s, g])
-
     for r in range(n_kv - 1):
         @pl.when(me == r)
         def _(r=r):
@@ -361,6 +345,17 @@
         grad_copy(xored(slot, d, half)).start()
     dk_ref[...] = key_grad
     dv_ref[...] = (folded_heads(dv_acc, rows) + landed[:, width:]).astype(jnp.bfloat16)
+
+    for d in range(half):
+        forward(d)
+
+    @pl.when(jnp.logical_not(native))
+    def _():
+        wait_for(x_all, x3_r)
+
+    for s in range(2):
+        for g in range(half):
+            x_t[s, g] = jnp.transpose(x_all[s, g])
 
     def row_sums(d, s):
         p = xored(slot, d, half)
@@ -430,6 +425,7 @@
         pltpu.VMEM((2, rows, width), bf16),
         pltpu.VMEM((log_sums.shape[1], rows), f32),
         pltpu.VMEM(chosen.shape, jnp.int32),
+        pltpu.VMEM((n_kv, 8, 128), jnp.int32),
         pltpu.VMEM((n_kv, 8, 128), jnp.int32),
         pltpu.VMEM((n_kv, KB, 2 * width), bf16),
         pltpu.VMEM((n_kv, KB, 2 * width), bf16),

time: 33.6 us -> 31.7 us (0.943)
  the two profiles are of different devices: /device:TPU:4 before, /device:TPU:0 now
where the time goes in v4:
time: 31.7 us; the launch traced here: 31.5 us
  Pallas kernels  30.9 us (97%)
  between operations  0.64 us (2%)
    pallas_call x1, Pallas kernels, per_device_fused(): pl.pallas_call(functools.partial(kernel, n_kv, n_tp), out_shape=tuple((pl...  30 us
    pallas_call x1, Pallas kernels, per_device_fused(): pl.pallas_call(put_out, out_shape=tuple((jax.ShapeDtypeStruct(shape, dtyp...  0.89 us

profile of v4, /device:TPU:0, one launch (start us, length us, event | category | flops | bytes accessed | tf_op | source)
XLA Modules:
  0.0 31.5 jit_solution(11878947474330735830)
XLA Ops:
  0.6 30.0 %shard_map.102 = (bf16[256,768]{1,0:T(8,128)(2,1)S(1)}, bf16[256,128]{1,0:T(8,128)(2,1)S(1)}, bf16[256,128]{1,0:T(8,128)(2,1)S(1)}, f32[384,128]{1,0:T(8,128)S(1)}) custom-call(bf16[256,768]{1,0:T(8,128)(2,1)} %q_hbm.1, bf16[256,128]{1,0:T(8,128)(2,1)} %k_hbm.1, bf16[256,128]{1,0:T(8,128)(2,1)} %v_hbm.1, f32[12,256]{1,0:T(8,128)} %bitcast.1, ...), custom_call_target="tpu_custom_call" | custom-call | tf_op jit(solution)/shard_map/pallas_call | solution.py:463
  30.6 0.9 %shard_map.103 = (bf16[256,768]{1,0:T(8,128)(2,1)}, bf16[256,128]{1,0:T(8,128)(2,1)}, bf16[256,128]{1,0:T(8,128)(2,1)}, f32[384,128]{1,0:T(8,128)}) custom-call(bf16[256,768]{1,0:T(8,128)(2,1)S(1)} %get-tuple-element.8.a, bf16[256,128]{1,0:T(8,128)(2,1)S(1)} %get-tuple-element.9.b, bf16[256,128]{1,0:T(8,128)(2,1)S(1)} %get-tuple-element.10.c, ...), custom_call_target="tpu_custom_call" | custom-call | tf_op jit(solution)/shard_map/pallas_call | solution.py:478

commit v5 on v4

--- a/solution.py
+++ b/solution.py
@@ -64,7 +64,7 @@
     q_hbm, k_hbm, v_hbm, lse_hbm, do_hbm, x_hbm, chosen_hbm,
     dq_ref, dk_ref, dv_ref, dw_ref,
     x_ref, qd_ref, kv_ref, lse_ref, chosen_ref, asking, asked, outgoing, fetched, ret_out, ret_in, x_all, x_t, kg_all, half_out, half_in, half_sum,
-    k_own, v_own, k_sel, v_sel, kt_own, kt_sel, bias_own, bias_sel, p_own, dp_own, delta, ds_sel,
+    k_own, v_own, k_sel, v_sel, kt_own, kt_sel, bias_own, bias_sel, p_own, dp_own, delta, ds_sel, p16_sel,
     dk_acc, dv_acc, dks_acc, dvs_acc, picks, picks_t,
     ask_s, ask_r, blk_s, blk_r, ret_r, x1_s, x1_r, x2_r, x3_r, xs_s, xf_s, kg_s, kg_r, half_s, half_r, in_s,
 ):
@@ -132,7 +132,10 @@
         return copy_to(outgoing.at[p], fetched.at[me], blk_s, blk_r, kv=p)
 
     def return_copy(o):
-        return copy_to(ret_out.at[o], ret_in.at[me], blk_s, ret_r, kv=o)
+        return copy_to(ret_out.at[0, o], ret_in.at[0, me], blk_s, ret_r.at[0], kv=o)
+
+    def return_values(o):
+        return copy_to(ret_out.at[1, o], ret_in.at[1, me], blk_s, ret_r.at[1], kv=o)
 
     def grad_copy(g):
         return copy_to(kg_all.at[slot], kg_all.at[slot], kg_s, kg_r.at[slot], kv=first + g)
@@ -140,20 +143,18 @@
     def half_copy():
         return copy_to(half_out, half_in, half_s, half_r, kv=mate)
 
-    def line_source(j):
-        return x_ref.at[:, pl.ds((j % per_tp) * feats, feats)]
-
     def start_lines():
-        for j in range(half):
-            mine = (j // per_tp) % cores == lax.rem(col, cores)
-
-            @pl.when(mine & (j != slot))
-            def _(j=j):
-                copy_to(line_source(j), x_all.at[side, slot], x1_s, x1_r.at[slot], kv=first + j).start()
-
-            @pl.when(mine & (j == slot))
-            def _(j=j):
-                pltpu.make_async_copy(line_source(j), x_all.at[side, slot], x1_r.at[j]).start()
+        for d in range(half):
+            p = xored(slot, d, half)
+            src = x_ref.at[:, pl.ds(pl.multiple_of(lax.rem(p, per_tp) * feats, 128), feats)]
+            mine = lax.rem(p // per_tp, cores) == lax.rem(col, cores)
+
+            @pl.when(mine)
+            def _(d=d, p=p, src=src):
+                if d == 0:
+                    pltpu.make_async_copy(src, x_all.at[side, slot], x1_r.at[slot]).start()
+                else:
+                    copy_to(src, x_all.at[side, slot], x1_s, x1_r.at[slot], kv=first + p).start()
 
     per_core = half // cores
     line_count = jnp.where(native, per_core - 1, per_core)
@@ -258,13 +259,20 @@
             axis=0,
         )
         ds_sel[m] = ds
+        p16_sel[m, :sel_rows] = first16
+        p16_sel[m, sel_rows:] = second16
         k_term = dot_nn(ds, q2)
-        v_term = dot_nn(jnp.concatenate([first16, second16], axis=0), do2)
         if m % per_head == 0:
             dks_acc[h] = k_term
+        else:
+            dks_acc[h] += k_term
+
+    def sel_values(m):
+        h = m // per_head
+        v_term = dot_nn(p16_sel[m], do_ref[:, lanes(m)])
+        if m % per_head == 0:
             dvs_acc[h] = v_term
         else:
-            dks_acc[h] += k_term
             dvs_acc[h] += v_term
 
     def own_pair_back(m):
@@ -310,6 +318,7 @@
 
     for d in range(1, half):
         spread(d)
+    forward(0)
     picks_t[...] = jnp.transpose(picks[...])
     for r in range(1, n_kv):
         @pl.when(me == r)
@@ -323,31 +332,38 @@
     for m in range(pairs):
         sel_pair(m)
 
-    ret_out[:, :, :width] = (
-        (folded_heads(dks_acc, sel_rows) * score_scale).astype(ret_out.dtype).reshape(n_kv, KB, width)
-    )
-    ret_out[:, :, width:] = folded_heads(dvs_acc, sel_rows).astype(ret_out.dtype).reshape(n_kv, KB, width)
+    ret_out[0] = (folded_heads(dks_acc, sel_rows) * score_scale).astype(ret_out.dtype).reshape(n_kv, KB, width)
     for o in reversed(range(n_kv)):
         @pl.when(o < me)
         def _(o=o):
             return_copy(o).start()
     for m in range(pairs):
         own_pair_back(m)
-    for r in range(n_kv - 1):
-        @pl.when(me == r)
-        def _(r=r):
-            wait_for(ret_in.at[pl.ds(r + 1, n_kv - 1 - r)], ret_r)
-
-    landed = dot_nn(picks_t[...], ret_in[...].reshape(sel_rows, 2 * width))
-    key_grad = (folded_heads(dk_acc, rows) * score_scale + landed[:, :width]).astype(jnp.bfloat16)
+    forward(1)
+    for m in range(pairs):
+        sel_values(m)
+    ret_out[1] = folded_heads(dvs_acc, sel_rows).astype(ret_out.dtype).reshape(n_kv, KB, width)
+    for o in range(n_kv):
+        @pl.when(o < me)
+        def _(o=o):
+            return_values(o).start()
+
+    def returned(side):
+        for r in range(n_kv - 1):
+            @pl.when(me == r)
+            def _(r=r):
+                wait_for(ret_in.at[side, pl.ds(r + 1, n_kv - 1 - r)], ret_r.at[side])
+
+        return dot_nn(picks_t[...], ret_in[side].reshape(sel_rows, width))
+
+    own_k = folded_heads(dk_acc, rows) * score_scale
+    for d in range(2, half):
+        forward(d)
+    key_grad = (own_k + returned(0)).astype(jnp.bfloat16)
     kg_all[slot] = key_grad
     for d in range(half - 1, 0, -1):
         grad_copy(xored(slot, d, half)).start()
     dk_ref[...] = key_grad
-    dv_ref[...] = (folded_heads(dv_acc, rows) + landed[:, width:]).astype(jnp.bfloat16)
-
-    for d in range(half):
-        forward(d)
 
     @pl.when(jnp.logical_not(native))
     def _():
@@ -373,6 +389,7 @@
     half_out[...] = (half_sum[...] + row_sums(half - 1, 1 - part_of)).astype(half_out.dtype)
     half_copy().start()
     dw_ref[...] += row_sums(half - 1, part_of)
+    dv_ref[...] = (folded_heads(dv_acc, rows) + returned(1)).astype(jnp.bfloat16)
     half_copy().wait_recv()
     dw_ref[...] += half_in[...].astype(jnp.float32)
 
@@ -429,8 +446,8 @@
         pltpu.VMEM((n_kv, 8, 128), jnp.int32),
         pltpu.VMEM((n_kv, KB, 2 * width), bf16),
         pltpu.VMEM((n_kv, KB, 2 * width), bf16),
-        pltpu.VMEM((n_kv, KB, 2 * width), bf16),
-        pltpu.VMEM((n_kv, KB, 2 * width), bf16),
+        pltpu.VMEM((2, n_kv, KB, width), bf16),
+        pltpu.VMEM((2, n_kv, KB, width), bf16),
         pltpu.VMEM((2, n_kv // 2, rows, feats), bf16),
         pltpu.VMEM((2, n_kv // 2, feats, rows), bf16),
         pltpu.VMEM((n_kv // 2, rows, width), bf16),
@@ -449,6 +466,7 @@
         pltpu.VMEM((pairs, 2 * rows, rows), f32),
         pltpu.VMEM((2 * pairs, rows), f32),
         pltpu.VMEM((pairs, 2 * sel_rows, rows), bf16),
+        pltpu.VMEM((pairs, 2 * sel_rows, rows), bf16),
         pltpu.VMEM((2, 2 * rows, width), f32),
         pltpu.VMEM((2, 2 * rows, width), f32),
         pltpu.VMEM((2, 2 * sel_rows, width), f32),
@@ -456,7 +474,7 @@
         pltpu.VMEM((sel_rows, rows), bf16),
         pltpu.VMEM((rows, sel_rows), bf16),
     ] + [
-        dma(()), dma(()), dma(()), dma(()), dma(()), dma(()), dma((n_kv // 2,)), dma((n_kv // 2,)), dma(()), dma(()),
+        dma(()), dma(()), dma(()), dma(()), dma((2,)), dma(()), dma((n_kv // 2,)), dma((n_kv // 2,)), dma(()), dma(()),
         dma(()), dma(()), dma((n_kv // 2,)), dma(()), dma(()), dma((5,)),
     ]
     shapes = (((rows, features), bf16), ((rows, width), bf16), ((rows, width), bf16), ((feats, width), f32))

time: 31.7 us -> 30.9 us (0.975)
  Pallas kernels: 30.9 us -> 30.1 us
    pallas_call x1, Pallas kernels: 30 us -> 29.2 us  [per_device_fused(): pl.pallas_call(functools.partial(kernel, n_kv, n_tp), out_shape=tuple((pl...]
where the time goes in v5:
time: 30.9 us; the launch traced here: 30.8 us
  Pallas kernels  30.1 us (97%)
  between operations  0.64 us (2%)
    pallas_call x1, Pallas kernels, per_device_fused(): pl.pallas_call(functools.partial(kernel, n_kv, n_tp), out_shape=tuple((pl...  29.2 us
    pallas_call x1, Pallas kernels, per_device_fused(): pl.pallas_call(put_out, out_shape=tuple((jax.ShapeDtypeStruct(shape, dtyp...  0.89 us

profile of v5, /device:TPU:0, one launch (start us, length us, event | category | flops | bytes accessed | tf_op | source)
XLA Modules:
  0.0 30.8 jit_solution(2548087583653978752)
XLA Ops:
  0.6 29.2 %shard_map.102 = (bf16[256,768]{1,0:T(8,128)(2,1)S(1)}, bf16[256,128]{1,0:T(8,128)(2,1)S(1)}, bf16[256,128]{1,0:T(8,128)(2,1)S(1)}, f32[384,128]{1,0:T(8,128)S(1)}) custom-call(bf16[256,768]{1,0:T(8,128)(2,1)} %q_hbm.1, bf16[256,128]{1,0:T(8,128)(2,1)} %k_hbm.1, bf16[256,128]{1,0:T(8,128)(2,1)} %v_hbm.1, f32[12,256]{1,0:T(8,128)} %bitcast.1, ...), custom_call_target="tpu_custom_call" | custom-call | tf_op jit(solution)/shard_map/pallas_call | solution.py:481
  29.9 0.9 %shard_map.103 = (bf16[256,768]{1,0:T(8,128)(2,1)}, bf16[256,128]{1,0:T(8,128)(2,1)}, bf16[256,128]{1,0:T(8,128)(2,1)}, f32[384,128]{1,0:T(8,128)}) custom-call(bf16[256,768]{1,0:T(8,128)(2,1)S(1)} %get-tuple-element.8.a, bf16[256,128]{1,0:T(8,128)(2,1)S(1)} %get-tuple-element.9.b, bf16[256,128]{1,0:T(8,128)(2,1)S(1)} %get-tuple-element.10.c, ...), custom_call_target="tpu_custom_call" | custom-call | tf_op jit(solution)/shard_map/pallas_call | solution.py:496

commit v6 on v5

--- a/solution.py
+++ b/solution.py
@@ -76,7 +76,9 @@
     per_head = pairs // 2
     here = rows // KB
     q_blocks = rows // QB
-    sel_rows = n_kv * KB
+    slots = n_kv - 1
+    sel_rows = slots * KB
+    all_rows = n_kv * KB
     feats = dw_ref.shape[0]
     per_tp = x_ref.shape[1] // feats
     mate = xored(me, n_kv // 2, n_kv)
@@ -308,7 +310,7 @@
     sender = lax.broadcasted_iota(jnp.int32, shape, 0)
     local = jnp.concatenate([jnp.concatenate([asked[...]] * (KB // 8), axis=1)] * (rows // 128), axis=2)
     chosen_here = (local >= 0) & (sender > me) & (at == local * KB)
-    picks[...] = jnp.where(chosen_here, 1.0, 0.0).astype(jnp.bfloat16).reshape(sel_rows, rows)
+    picks[...] = jnp.where(chosen_here, 1.0, 0.0).astype(jnp.bfloat16).reshape(all_rows, rows)
     both = jnp.concatenate([k_ref[...], v_ref[...]], axis=1)
     outgoing[...] = dot_nn(picks[...], both).astype(jnp.bfloat16).reshape(n_kv, KB, 2 * width)
     for p in reversed(range(n_kv)):
@@ -332,8 +334,8 @@
     for m in range(pairs):
         sel_pair(m)
 
-    ret_out[0] = (folded_heads(dks_acc, sel_rows) * score_scale).astype(ret_out.dtype).reshape(n_kv, KB, width)
-    for o in reversed(range(n_kv)):
+    ret_out[0] = (folded_heads(dks_acc, sel_rows) * score_scale).astype(ret_out.dtype).reshape(slots, KB, width)
+    for o in reversed(range(slots)):
         @pl.when(o < me)
         def _(o=o):
             return_copy(o).start()
@@ -342,8 +344,8 @@
     forward(1)
     for m in range(pairs):
         sel_values(m)
-    ret_out[1] = folded_heads(dvs_acc, sel_rows).astype(ret_out.dtype).reshape(n_kv, KB, width)
-    for o in range(n_kv):
+    ret_out[1] = folded_heads(dvs_acc, sel_rows).astype(ret_out.dtype).reshape(slots, KB, width)
+    for o in range(slots):
         @pl.when(o < me)
         def _(o=o):
             return_values(o).start()
@@ -354,16 +356,21 @@
             def _(r=r):
                 wait_for(ret_in.at[side, pl.ds(r + 1, n_kv - 1 - r)], ret_r.at[side])
 
-        return dot_nn(picks_t[...], ret_in[side].reshape(sel_rows, width))
+        return dot_nn(picks_t[...], ret_in[side].reshape(all_rows, width))
 
     own_k = folded_heads(dk_acc, rows) * score_scale
-    for d in range(2, half):
-        forward(d)
+    def last_forwards():
+        for d in range(2, half):
+            forward(d)
+
+    pl.when(part_of == 0)(last_forwards)
     key_grad = (own_k + returned(0)).astype(jnp.bfloat16)
     kg_all[slot] = key_grad
-    for d in range(half - 1, 0, -1):
+    for d in range(1, half):
         grad_copy(xored(slot, d, half)).start()
     dk_ref[...] = key_grad
+
+    pl.when(part_of != 0)(last_forwards)
 
     @pl.when(jnp.logical_not(native))
     def _():
@@ -377,18 +384,18 @@
         p = xored(slot, d, half)
         return dot_nn(x_t[s, p], kg_all[p])
 
-    theirs, ours = row_sums(0, 1 - part_of), row_sums(0, part_of)
-    half_sum[...] = theirs
-    dw_ref[...] = ours
+    half_sum[...] = row_sums(0, 1 - part_of)
     for d in range(1, half):
         g = xored(slot, d, half)
         wait_for(kg_all.at[g], kg_r.at[g])
         if d < half - 1:
             half_sum[...] += row_sums(d, 1 - part_of)
-            dw_ref[...] += row_sums(d, part_of)
     half_out[...] = (half_sum[...] + row_sums(half - 1, 1 - part_of)).astype(half_out.dtype)
     half_copy().start()
-    dw_ref[...] += row_sums(half - 1, part_of)
+    ours = row_sums(0, part_of)
+    for d in range(1, half):
+        ours = ours + row_sums(d, part_of)
+    dw_ref[...] = ours
     dv_ref[...] = (folded_heads(dv_acc, rows) + returned(1)).astype(jnp.bfloat16)
     half_copy().wait_recv()
     dw_ref[...] += half_in[...].astype(jnp.float32)
@@ -397,7 +404,7 @@
         @pl.when(me == r)
         def _(r=r):
             wait_for(asked.at[pl.ds(0, r)], ask_s)
-    wait_for(fetched.at[pl.ds(0, n_kv - 1)], blk_s)
+    wait_for(fetched, blk_s)
     wait_for(kg_all.at[pl.ds(0, half - 1)], kg_s)
     for count in range(1, half + 1):
         @pl.when(line_count == count)
@@ -413,10 +420,10 @@
 
 
 def put_out(a, b, c, d, a_out, b_out, c_out, d_out, sems):
-    copies = [
-        pltpu.make_async_copy(src, dst, sems.at[n])
-        for n, (src, dst) in enumerate([(a, a_out), (b, b_out), (c, c_out), (d, d_out)])
-    ]
+    quarter = a.shape[0] // 4
+    parts = [(a.at[pl.ds(n * quarter, quarter)], a_out.at[pl.ds(n * quarter, quarter)]) for n in range(4)]
+    parts += [(d, d_out), (b, b_out), (c, c_out)]
+    copies = [pltpu.make_async_copy(src, dst, sems.at[n]) for n, (src, dst) in enumerate(parts)]
     for copy in copies:
         copy.start()
     for copy in copies:
@@ -429,7 +436,8 @@
     rows, features = queries.shape
     width = key_vectors.shape[1]
     pairs = features // width
-    sel_rows = n_kv * KB
+    sel_rows = (n_kv - 1) * KB
+    all_rows = n_kv * KB
     feats = layer_input.shape[1] * n_tp // n_kv
     per_tp = layer_input.shape[1] // feats
     f32, bf16 = jnp.float32, jnp.bfloat16
@@ -445,8 +453,8 @@
         pltpu.VMEM((n_kv, 8, 128), jnp.int32),
         pltpu.VMEM((n_kv, 8, 128), jnp.int32),
         pltpu.VMEM((n_kv, KB, 2 * width), bf16),
-        pltpu.VMEM((n_kv, KB, 2 * width), bf16),
-        pltpu.VMEM((2, n_kv, KB, width), bf16),
+        pltpu.VMEM((n_kv - 1, KB, 2 * width), bf16),
+        pltpu.VMEM((2, n_kv - 1, KB, width), bf16),
         pltpu.VMEM((2, n_kv, KB, width), bf16),
         pltpu.VMEM((2, n_kv // 2, rows, feats), bf16),
         pltpu.VMEM((2, n_kv // 2, feats, rows), bf16),
@@ -471,8 +479,8 @@
         pltpu.VMEM((2, 2 * rows, width), f32),
         pltpu.VMEM((2, 2 * sel_rows, width), f32),
         pltpu.VMEM((2, 2 * sel_rows, width), f32),
-        pltpu.VMEM((sel_rows, rows), bf16),
-        pltpu.VMEM((rows, sel_rows), bf16),
+        pltpu.VMEM((all_rows, rows), bf16),
+        pltpu.VMEM((rows, all_rows), bf16),
     ] + [
         dma(()), dma(()), dma(()), dma(()), dma((2,)), dma(()), dma((n_kv // 2,)), dma((n_kv // 2,)), dma(()), dma(()),
         dma(()), dma(()), dma((n_kv // 2,)), dma(()), dma(()), dma((5,)),
@@ -498,7 +506,7 @@
         out_shape=tuple(jax.ShapeDtypeStruct(shape, dtype) for shape, dtype in shapes),
         in_specs=[vmem] * 4,
         out_specs=(hbm,) * 4,
-        scratch_shapes=[dma((4,))],
+        scratch_shapes=[dma((7,))],
         compiler_params=pltpu.CompilerParams(vmem_limit_bytes=8 << 20),
     )(*(pltpu.with_memory_space_constraint(x, pltpu.VMEM) for x in held))
 

time: 30.9 us -> 30.3 us (0.981)
  Pallas kernels: 30.1 us -> 29.5 us
    pallas_call x1, Pallas kernels: 29.2 us -> 28.6 us  [per_device_fused(): pl.pallas_call(functools.partial(kernel, n_kv, n_tp), out_shape=tuple((pl...]
where the time goes in v6:
time: 30.3 us; the launch traced here: 30.1 us
  Pallas kernels  29.5 us (97%)
  between operations  0.64 us (2%)
    pallas_call x1, Pallas kernels, per_device_fused(): pl.pallas_call(functools.partial(kernel, n_kv, n_tp), out_shape=tuple((pl...  28.6 us
    pallas_call x1, Pallas kernels, per_device_fused(): pl.pallas_call(put_out, out_shape=tuple((jax.ShapeDtypeStruct(shape, dtyp...  0.91 us

profile of v6, /device:TPU:0, one launch (start us, length us, event | category | flops | bytes accessed | tf_op | source)
XLA Modules:
  0.0 30.1 jit_solution(16493886476457838313)
XLA Ops:
  0.6 28.6 %shard_map.102 = (bf16[256,768]{1,0:T(8,128)(2,1)S(1)}, bf16[256,128]{1,0:T(8,128)(2,1)S(1)}, bf16[256,128]{1,0:T(8,128)(2,1)S(1)}, f32[384,128]{1,0:T(8,128)S(1)}) custom-call(bf16[256,768]{1,0:T(8,128)(2,1)} %q_hbm.1, bf16[256,128]{1,0:T(8,128)(2,1)} %k_hbm.1, bf16[256,128]{1,0:T(8,128)(2,1)} %v_hbm.1, f32[12,256]{1,0:T(8,128)} %bitcast.1, ...), custom_call_target="tpu_custom_call" | custom-call | tf_op jit(solution)/shard_map/pallas_call | solution.py:489
  29.2 0.9 %shard_map.103 = (bf16[256,768]{1,0:T(8,128)(2,1)}, bf16[256,128]{1,0:T(8,128)(2,1)}, bf16[256,128]{1,0:T(8,128)(2,1)}, f32[384,128]{1,0:T(8,128)}) custom-call(bf16[256,768]{1,0:T(8,128)(2,1)S(1)} %get-tuple-element.8.a, bf16[256,128]{1,0:T(8,128)(2,1)S(1)} %get-tuple-element.9.b, bf16[256,128]{1,0:T(8,128)(2,1)S(1)} %get-tuple-element.10.c, ...), custom_call_target="tpu_custom_call" | custom-call | tf_op jit(solution)/shard_map/pallas_call | solution.py:504

commit v7 on v6

--- a/solution.py
+++ b/solution.py
@@ -81,14 +81,19 @@
     all_rows = n_kv * KB
     feats = dw_ref.shape[0]
     per_tp = x_ref.shape[1] // feats
-    mate = xored(me, n_kv // 2, n_kv)
+    mate = n_kv // 2 * (1 - me // (n_kv // 2)) + xored(lax.rem(me, n_kv // 2), n_kv // 4, n_kv // 2)
     half = n_kv // 2
     cores = n_tp // 2
     slot = lax.rem(me, half)
     first = me - slot
     part_of = me // half
     side = col // cores
-    native = lax.rem(me // per_tp, cores) == lax.rem(col, cores)
+    swap = jnp.where(side == part_of, 0, 1)
+
+    def holds(p):
+        return lax.rem(p // per_tp + swap, cores) == lax.rem(col, cores)
+
+    native = holds(slot)
     twin = xored(col, 1, n_tp)
     score_scale = HEAD ** (-0.5)
 
@@ -149,9 +154,8 @@
         for d in range(half):
             p = xored(slot, d, half)
             src = x_ref.at[:, pl.ds(pl.multiple_of(lax.rem(p, per_tp) * feats, 128), feats)]
-            mine = lax.rem(p // per_tp, cores) == lax.rem(col, cores)
-
-            @pl.when(mine)
+
+            @pl.when(holds(p))
             def _(d=d, p=p, src=src):
                 if d == 0:
                     pltpu.make_async_copy(src, x_all.at[side, slot], x1_r.at[slot]).start()
@@ -174,7 +178,7 @@
     def forward(d):
         p = xored(slot, d, half)
 
-        @pl.when(native)
+        @pl.when(jnp.logical_not(native))
         def _():
             wait_for(x_all.at[1 - side, p], x2_r.at[p])
             copy_to(x_all.at[1 - side, p], x_all.at[1 - side, p], xf_s, x3_r, tp=twin).start()
@@ -318,8 +322,13 @@
         def _(p=p):
             block_copy(p).start()
 
-    for d in range(1, half):
-        spread(d)
+    def neighbour_spreads():
+        for d in range(2, half):
+            spread(d)
+
+    hurried = (part_of != 0)
+    spread(1)
+    pl.when(jnp.logical_not(hurried))(neighbour_spreads)
     forward(0)
     picks_t[...] = jnp.transpose(picks[...])
     for r in range(1, n_kv):
@@ -339,16 +348,20 @@
         @pl.when(o < me)
         def _(o=o):
             return_copy(o).start()
+    pl.when(hurried)(neighbour_spreads)
     for m in range(pairs):
         own_pair_back(m)
     forward(1)
     for m in range(pairs):
         sel_values(m)
     ret_out[1] = folded_heads(dvs_acc, sel_rows).astype(ret_out.dtype).reshape(slots, KB, width)
-    for o in range(slots):
-        @pl.when(o < me)
-        def _(o=o):
-            return_values(o).start()
+    def send_values():
+        for o in range(slots):
+            @pl.when(o < me)
+            def _(o=o):
+                return_values(o).start()
+
+    pl.when(part_of == 0)(send_values)
 
     def returned(side):
         for r in range(n_kv - 1):
@@ -366,15 +379,20 @@
     pl.when(part_of == 0)(last_forwards)
     key_grad = (own_k + returned(0)).astype(jnp.bfloat16)
     kg_all[slot] = key_grad
-    for d in range(1, half):
-        grad_copy(xored(slot, d, half)).start()
+    def send_grads(order):
+        for g in order:
+            @pl.when(g != slot)
+            def _(g=g):
+                grad_copy(g).start()
+
+    pl.when(part_of == 0)(lambda: send_grads([*range(half // 2, half), *reversed(range(half // 2))]))
+    pl.when(part_of != 0)(lambda: send_grads(range(half)))
     dk_ref[...] = key_grad
 
+    pl.when(part_of != 0)(send_values)
     pl.when(part_of != 0)(last_forwards)
 
-    @pl.when(jnp.logical_not(native))
-    def _():
-        wait_for(x_all, x3_r)
+    wait_for(x_all.at[0], x3_r)
 
     for s in range(2):
         for g in range(half):
@@ -411,11 +429,8 @@
         def _(count=count):
             wait_for(x_all.at[0, pl.ds(0, count)], x1_s)
 
-    @pl.when(native)
-    def _():
-        wait_for(x_all.at[0], xs_s)
-        wait_for(x_all, xf_s)
-
+    pl.when(native)(lambda: wait_for(x_all.at[0], xs_s))
+    wait_for(x_all.at[0], xf_s)
     half_copy().wait_send()
 
 

time: 30.3 us -> 30 us (0.990)
  Pallas kernels: 29.5 us -> 29.1 us
    pallas_call x1, Pallas kernels: 28.6 us -> 28.2 us  [per_device_fused(): pl.pallas_call(functools.partial(kernel, n_kv, n_tp), out_shape=tuple((pl...]
where the time goes in v7:
time: 30 us; the launch traced here: 29.8 us
  Pallas kernels  29.1 us (97%)
  between operations  0.64 us (2%)
    pallas_call x1, Pallas kernels, per_device_fused(): pl.pallas_call(functools.partial(kernel, n_kv, n_tp), out_shape=tuple((pl...  28.2 us
    pallas_call x1, Pallas kernels, per_device_fused(): pl.pallas_call(put_out, out_shape=tuple((jax.ShapeDtypeStruct(shape, dtyp...  0.91 us

profile of v7, /device:TPU:0, one launch (start us, length us, event | category | flops | bytes accessed | tf_op | source)
XLA Modules:
  0.0 29.8 jit_solution(4331659953304485831)
XLA Ops:
  0.6 28.2 %shard_map.102 = (bf16[256,768]{1,0:T(8,128)(2,1)S(1)}, bf16[256,128]{1,0:T(8,128)(2,1)S(1)}, bf16[256,128]{1,0:T(8,128)(2,1)S(1)}, f32[384,128]{1,0:T(8,128)S(1)}) custom-call(bf16[256,768]{1,0:T(8,128)(2,1)} %q_hbm.1, bf16[256,128]{1,0:T(8,128)(2,1)} %k_hbm.1, bf16[256,128]{1,0:T(8,128)(2,1)} %v_hbm.1, f32[12,256]{1,0:T(8,128)} %bitcast.1, ...), custom_call_target="tpu_custom_call" | custom-call | tf_op jit(solution)/shard_map/pallas_call | solution.py:504
  28.9 0.9 %shard_map.103 = (bf16[256,768]{1,0:T(8,128)(2,1)}, bf16[256,128]{1,0:T(8,128)(2,1)}, bf16[256,128]{1,0:T(8,128)(2,1)}, f32[384,128]{1,0:T(8,128)}) custom-call(bf16[256,768]{1,0:T(8,128)(2,1)S(1)} %get-tuple-element.8.a, bf16[256,128]{1,0:T(8,128)(2,1)S(1)} %get-tuple-element.9.b, bf16[256,128]{1,0:T(8,128)(2,1)S(1)} %get-tuple-element.10.c, ...), custom_call_target="tpu_custom_call" | custom-call | tf_op jit(solution)/shard_map/pallas_call | solution.py:519
